TPU v7x, 512 devices: a 4x2x32 block of a 4x8x32 slice. The times are simulated.
512 devices in a mesh: grp: 2 (over y), sp: 64 (over z, core), tp: 4 (over x).
Axes of the slice: x: 4, y: 2, z: 32, core: 2. Of those that a mesh axis runs over, the one named last changes fastest.
The devices are a block of a 4x8x32 slice.
Arguments:
- tokens: bfloat16 [32768, 4096], P(('grp', 'sp'), 'tp'), parts along dimension 0, may hold values from -45 to 45
- norm_gain: float32 [2, 4096], replicated, may hold values from 0.1 to 1.9
- value_weight: bfloat16 [2, 4096, 1024], P(None, 'sp', 'tp'), may hold values from -0.09375 to 0.09375
- gate_weight: bfloat16 [2, 4096, 1024], P(None, 'sp', 'tp'), may hold values from -0.09375 to 0.09375
- conv_taps: float32 [2, 31, 1024], P(None, None, 'tp'), may hold values from -4 to 4
- channel_gain: float32 [2, 1024], P(None, 'tp'), may hold values from 0.1 to 1.9
- out_weight: bfloat16 [2, 1024, 4096], P(None, 'sp', 'tp'), may hold values from -0.375 to 0.375
- final_gain: float32 [4096], P('tp'), may hold values from 0.1 to 1.9
Outputs:
- result: bfloat16 [32768, 4096], P(('grp', 'sp'), 'tp'), parts along dimension 0
There are 2 independent parts, one for each index of `grp`. A program takes and returns all parts, laid end to end along the dimension named above; an argument that names none is the same for every part. Nothing has to cross between parts.
All inputs are finite; a program needn't handle non-finite values.
Results may differ from a plain program's by a relative error of at most 0.012.
Values may be sent and summed in bfloat16 or wider, within the bound.
No kernel may reach another device: no remote copies, remote signals or barrier semaphores. Data moves between devices by JAX's collectives and lax.ppermute only.
A program may use at most 128 MiB of HBM per device.

v0:
```python
import jax
import jax.numpy as jnp
from jax import lax
from jax.sharding import PartitionSpec as P

D = 4096
C = 1024
LAYERS = 2


def joined_along(pieces, dim):
    dims = list(pieces.shape[1:])
    dims[dim] *= pieces.shape[0]
    return jnp.moveaxis(pieces, 0, dim).reshape(dims)


def one_gather(arrays, axis, dims):
    ravelled = jnp.concatenate([a.reshape(-1) for a in arrays])
    lines, at, finished = (lax.all_gather(ravelled, axis), 0, [])
    for a, dim in zip(arrays, dims):
        pieces = lines[:, at : at + a.size].reshape(-1, *a.shape)
        finished.append(joined_along(pieces, dim))
        at += a.size
    return tuple(finished)


def copy_for_each(value, axis):
    size = lax.axis_size(axis)
    return lax.all_to_all(
        jnp.broadcast_to(value[None], (size, *value.shape)), axis, 0, 0, tiled=True
    )


def gather_directly(value, axis, dim):
    pieces = copy_for_each(value, axis)
    return joined_along(pieces, dim)


def with_halo(block, sides, width):
    for axis, dim in sides:
        count = lax.axis_size(axis)
        forward = [(i, i + 1) for i in range(count - 1)]
        backward = [(target, source) for source, target in forward]
        low = lax.ppermute(
            lax.slice_in_dim(block, block.shape[dim] - width, None, axis=dim), axis, forward
        )
        high = lax.ppermute(lax.slice_in_dim(block, 0, width, axis=dim), axis, backward)
        block = jnp.concatenate([low, block, high], axis=dim)
    return block


def over_copies(value, axis):
    everything = copy_for_each(value, axis)
    return jnp.sum(everything, axis=0)


def packed_total(arrays, axis):
    ravelled, at, finished = (jnp.concatenate([a.reshape(-1) for a in arrays]), 0, [])
    subtotal = over_copies(ravelled, axis)
    for a in arrays:
        finished.append(subtotal[at : at + a.size].reshape(a.shape))
        at += a.size
    return tuple(finished)


def on_device(
    tokens, norm_gain, value_weight, gate_weight, conv_taps, channel_gain, out_weight, final_gain
):
    rows = tokens.shape[0]
    chan_local = channel_gain.shape[1]
    x_state = tokens
    value_all, gate_all, out_all = one_gather(
        (value_weight, gate_weight, out_weight), "sp", (1, 1, 1)
    )
    for layer in range(LAYERS):
        xf = x_state.astype(jnp.float32)
        whole = gather_directly(x_state, "tp", 1).astype(jnp.float32)
        scale = lax.rsqrt(jnp.mean(whole * whole, axis=1, keepdims=True) + 1e-06)
        normed = (whole * scale * norm_gain[layer][None, :]).astype(jnp.bfloat16)
        value = jnp.dot(normed, value_all[layer], preferred_element_type=jnp.float32)
        gate = jnp.dot(normed, gate_all[layer], preferred_element_type=jnp.float32)
        glu = (value * jax.nn.sigmoid(gate)).astype(jnp.bfloat16)
        taps = conv_taps[layer]
        reach = taps.shape[0] // 2
        padded = with_halo(glu, (("sp", 0),), reach).astype(jnp.float32)
        conv = jnp.zeros((rows, chan_local), jnp.float32)
        for tap in range(taps.shape[0]):
            conv = conv + taps[tap][None, :] * padded[tap : tap + rows]
        sums, square_sums = packed_total(
            (jnp.sum(conv, axis=1), jnp.sum(conv * conv, axis=1)), "tp"
        )
        center = sums / C
        spread = square_sums / C - center * center
        normal_conv = (conv - center[:, None]) * lax.rsqrt(spread + 1e-05)[:, None]
        act_local = jax.nn.silu(normal_conv * channel_gain[layer][None, :]).astype(jnp.bfloat16)
        act = gather_directly(act_local, "tp", 1)
        branch = jnp.dot(act, out_all[layer], preferred_element_type=jnp.float32)
        x_state = (xf + branch).astype(jnp.bfloat16)
    xf = x_state.astype(jnp.float32)
    squares = over_copies(jnp.sum(xf * xf, axis=1), "tp")
    scale = lax.rsqrt(squares / D + 1e-06)[:, None]
    return (xf * scale * final_gain[None, :]).astype(jnp.bfloat16)


def solution(mesh):
    placed = (
        P(("grp", "sp"), "tp"),
        P(),
        P(None, "sp", "tp"),
        P(None, "sp", "tp"),
        P(None, None, "tp"),
        P(None, "tp"),
        P(None, "sp", "tp"),
        P("tp"),
    )
    return jax.shard_map(
        on_device, mesh=mesh, in_specs=placed, out_specs=P(("grp", "sp"), "tp"), check_vma=False
    )
```

profile of v0, /device:TPU:40, one launch (start us, length us, event | category | flops | bytes accessed | tf_op | source)
XLA Modules:
  0.0 323.7 jit_solution(254623838276804751)
XLA Ops:
  6.6 0.9 copy.35
  7.4 0.9 copy.36
  8.3 0.9 copy.37
  9.2 0.7 pad_maximum_fusion
  9.9 1.2 copy.21
  11.2 1.5 broadcast_in_dim.14
  12.7 4.7 %all-to-all-start = ((bf16[4,256,1024]{1,2,0:T(8,128)(2,1)}), bf16[4,256,1024]{1,2,0:T(8,128)(2,1)S(1)}, u32[]{:S(2)}, u32[]{:S(2)}) async-start(bf16[4,256,1024]{1,2,0:T(8,128)(2,1)} %broadcast_in_dim.14), calls=%async_computation | async-start | bytes 4194304 | tf_op jit(solution)/shard_map/all_to_all | solution.py:29
  17.6 26.2 %all-to-all-done = bf16[4,256,1024]{1,2,0:T(8,128)(2,1)S(1)} async-done(((bf16[4,256,1024]{1,2,0:T(8,128)(2,1)}), bf16[4,256,1024]{1,2,0:T(8,128)(2,1)S(1)}, u32[]{:S(2)}, u32[]{:S(2)}) %all-to-all-start) | async-done | bytes 2097184 | tf_op jit(solution)/shard_map/all_to_all | solution.py:29
  44.4 1.7 fusion.2
  46.1 135.0 %all-gather.3.cloned.1.call-done = bf16[6291456]{0:T(1024)(128)(2,1)} async-done(((bf16[98304]{0:T(1024)(128)(2,1)}), bf16[6291456]{0:T(1024)(128)(2,1)}) %all-gather.3.cloned.1.call-update) | async-done | bytes 12582928 | tf_op jit(solution)/shard_map/all_gather | solution.py:19
  181.1 13.5 %reshape.265 = bf16[64,98304]{1,0:T(8,128)(2,1)} reshape(bf16[6291456]{0:T(1024)(128)(2,1)} %all-gather.3.cloned.1.call-done) | data formatting | bytes 25165824 | tf_op jit(solution)/shard_map/all_gather | solution.py:19
  194.6 7.0 %fusion.85 = (bf16[64,32768]{1,0:T(8,128)(2,1)}, bf16[64,32768]{1,0:T(8,128)(2,1)S(1)}, bf16[64,32768]{1,0:T(8,128)(2,1)S(1)}) fusion(bf16[64,98304]{1,0:T(8,128)(2,1)} %reshape.265), kind=kLoop, calls=%fused_computation.173 | loop fusion | bytes 25165824 | tf_op jit(solution)/shard_map/slice | solution.py:21
  201.6 1.1 copy.39
  202.7 1.6 fusion.87
  204.4 1.1 copy.38
  205.5 1.8 fusion.88
  207.5 0.8 fusion.96
  208.2 0.8 fusion.16
  209.1 2.2 collective-permute-start
  211.2 1.3 collective-permute-start.1
  212.6 1.8 collective-permute-done.1
  214.4 1.1 fusion.82
  216.1 4.2 %all-to-all-start.1 = ((f32[4,1,512]{2,1,0:T(1,128)}), f32[4,1,512]{2,1,0:T(1,128)S(1)}, u32[]{:S(2)}, u32[]{:S(2)}) async-start(f32[4,1,512]{2,1,0:T(1,128)} %broadcast_in_dim.15), calls=%async_computation.1 | async-start | bytes 16384 | tf_op jit(solution)/shard_map/all_to_all | solution.py:29
  220.3 5.3 %all-to-all-done.1 = f32[4,1,512]{2,1,0:T(1,128)S(1)} async-done(((f32[4,1,512]{2,1,0:T(1,128)}), f32[4,1,512]{2,1,0:T(1,128)S(1)}, u32[]{:S(2)}, u32[]{:S(2)}) %all-to-all-start.1) | async-done | bytes 8224 | tf_op jit(solution)/shard_map/all_to_all | solution.py:29
  226.0 0.8 broadcast_in_dim.16
  226.8 3.7 %all-to-all-start.2 = ((bf16[4,256,256]{1,2,0:T(8,128)(2,1)}), bf16[4,256,256]{1,2,0:T(8,128)(2,1)S(1)}, u32[]{:S(2)}, u32[]{:S(2)}) async-start(bf16[4,256,256]{1,2,0:T(8,128)(2,1)} %broadcast_in_dim.16), calls=%async_computation.2 | async-start | bytes 1048576 | tf_op jit(solution)/shard_map/all_to_all | solution.py:29
  230.5 4.7 %copy.40 = bf16[8,8,32,1024]{3,2,1,0:T(8,128)(2,1)S(1)} copy(bf16[8,8,32,1024]{3,1,2,0:T(8,128)(2,1)} %bitcast.118) | data formatting | bytes 8388608
  235.2 1.8 fusion.86
  237.0 4.1 %all-to-all-done.2 = bf16[4,256,256]{1,2,0:T(8,128)(2,1)S(1)} async-done(((bf16[4,256,256]{1,2,0:T(8,128)(2,1)}), bf16[4,256,256]{1,2,0:T(8,128)(2,1)S(1)}, u32[]{:S(2)}, u32[]{:S(2)}) %all-to-all-start.2) | async-done | bytes 524320 | tf_op jit(solution)/shard_map/all_to_all | solution.py:29
  241.2 0.8 copy-done.3
  241.9 1.8 fusion.6
  243.9 1.4 broadcast_in_dim.17
  245.4 3.7 %all-to-all-start.3 = ((bf16[4,256,1024]{1,2,0:T(8,128)(2,1)}), bf16[4,256,1024]{1,2,0:T(8,128)(2,1)S(1)}, u32[]{:S(2)}, u32[]{:S(2)}) async-start(bf16[4,256,1024]{1,2,0:T(8,128)(2,1)} %broadcast_in_dim.17), calls=%async_computation.3 | async-start | bytes 4194304 | tf_op jit(solution)/shard_map/all_to_all | solution.py:29
  249.1 26.8 %all-to-all-done.3 = bf16[4,256,1024]{1,2,0:T(8,128)(2,1)S(1)} async-done(((bf16[4,256,1024]{1,2,0:T(8,128)(2,1)}), bf16[4,256,1024]{1,2,0:T(8,128)(2,1)S(1)}, u32[]{:S(2)}, u32[]{:S(2)}) %all-to-all-start.3) | async-done | bytes 2097184 | tf_op jit(solution)/shard_map/all_to_all | solution.py:29
  276.5 0.7 fusion.5
  277.2 0.9 copy-done.5
  278.1 0.7 fusion.97
  278.8 0.8 copy-done.4
  279.7 0.8 fusion.17
  280.4 1.3 collective-permute-start.2
  281.8 1.3 collective-permute-start.3
  283.1 1.8 collective-permute-done.3
  284.9 1.1 fusion.81
  286.1 7.8 %all_to_all.38 = f32[4,1,512]{2,1,0:T(1,128)S(1)} all-to-all(f32[4,1,512]{2,1,0:T(1,128)S(1)} %broadcast_in_dim.18), channel_id=1, replica_groups=mesh['grp'=2,'sp'=64,'tp'=4] {'tp'}, dimensions={0} | all-to-all | bytes 16384 | tf_op jit(solution)/shard_map/all_to_all | solution.py:29
  294.3 13.0 %all_to_all.39 = bf16[4,256,256]{1,2,0:T(8,128)(2,1)S(1)} all-to-all(bf16[4,256,256]{1,2,0:T(8,128)(2,1)S(1)} %broadcast_in_dim.19), channel_id=1, replica_groups=mesh['grp'=2,'sp'=64,'tp'=4] {'tp'}, dimensions={0} | all-to-all | bytes 1048576 | tf_op jit(solution)/shard_map/all_to_all | solution.py:29
  307.3 0.8 fusion.18
  308.2 7.7 %all_to_all.40 = f32[4,1,256]{2,1,0:T(1,128)S(1)} all-to-all(f32[4,1,256]{2,1,0:T(1,128)S(1)} %broadcast_in_dim.20), channel_id=1, replica_groups=mesh['grp'=2,'sp'=64,'tp'=4] {'tp'}, dimensions={0} | all-to-all | bytes 8192 | tf_op jit(solution)/shard_map/all_to_all | solution.py:29
  315.9 1.0 fusion.20
  (54 shorter events, 3.3 us)
Async XLA Ops:
  6.5 174.5 %all-gather.3.cloned.1.call-start = ((), (), s32[]{:S(2)}) async-start(), calls=%async_computation.7 | async-start | bytes 12779520 | tf_op jit(solution)/shard_map/all_gather | solution.py:19
  12.7 4.7 %copy-start.7 = (f32[2,4096]{1,0:T(2,128)S(1)}, f32[2,4096]{1,0:T(2,128)}, u32[]{:S(2)}) copy-start(f32[2,4096]{1,0:T(2,128)} %param.9) | copy-start | bytes 98308
  12.7 4.8 %copy-start.6 = (f32[2,31,256]{2,0,1:T(2,128)S(1)}, f32[2,31,256]{2,0,1:T(2,128)}, u32[]{:S(2)}) copy-start(f32[2,31,256]{2,0,1:T(2,128)} %param.12) | copy-start | bytes 190468
  12.7 31.1 %all-to-all-start = ((bf16[4,256,1024]{1,2,0:T(8,128)(2,1)}), bf16[4,256,1024]{1,2,0:T(8,128)(2,1)S(1)}, u32[]{:S(2)}, u32[]{:S(2)}) async-start(bf16[4,256,1024]{1,2,0:T(8,128)(2,1)} %broadcast_in_dim.14), calls=%async_computation | async-start | bytes 4194304 | tf_op jit(solution)/shard_map/all_to_all | solution.py:29
  205.5 2.0 copy-start.1
  209.1 3.5 %collective-permute-start = (bf16[15,256]{1,0:T(8,128)(2,1)S(1)}, bf16[15,256]{1,0:T(8,128)(2,1)S(1)}, u32[]{:S(2)}, u32[]{:S(2)}) collective-permute-start(bf16[15,256]{1,0:T(8,128)(2,1)S(1)} %get-tuple-element.24), channel_id=1, source_target_pairs={{0,4},{4,8},{8,12},{12,16},{16,20},{20,24},{24,28},{28,32},{32,36}... | collective-permute-start | bytes 23048 | tf_op jit(solution)/shard_map/ppermute | solution.py:44
  211.2 3.1 collective-permute-start.1
  214.4 6.0 %copy-start.9 = (f32[2,256]{1,0:T(2,128)S(1)}, f32[2,256]{1,0:T(2,128)}, u32[]{:S(2)}) copy-start(f32[2,256]{1,0:T(2,128)} %param.13) | copy-start | bytes 6148
  216.1 9.5 %all-to-all-start.1 = ((f32[4,1,512]{2,1,0:T(1,128)}), f32[4,1,512]{2,1,0:T(1,128)S(1)}, u32[]{:S(2)}, u32[]{:S(2)}) async-start(f32[4,1,512]{2,1,0:T(1,128)} %broadcast_in_dim.15), calls=%async_computation.1 | async-start | bytes 16384 | tf_op jit(solution)/shard_map/all_to_all | solution.py:29
  226.8 14.4 %all-to-all-start.2 = ((bf16[4,256,256]{1,2,0:T(8,128)(2,1)}), bf16[4,256,256]{1,2,0:T(8,128)(2,1)S(1)}, u32[]{:S(2)}, u32[]{:S(2)}) async-start(bf16[4,256,256]{1,2,0:T(8,128)(2,1)} %broadcast_in_dim.16), calls=%async_computation.2 | async-start | bytes 1048576 | tf_op jit(solution)/shard_map/all_to_all | solution.py:29
  235.2 6.8 %copy-start.2 = (bf16[256,1024]{1,0:T(8,128)(2,1)S(1)}, bf16[256,1024]{1,0:T(8,128)(2,1)}, u32[]{:S(2)}) copy-start(bf16[256,1024]{1,0:T(8,128)(2,1)} %param.8) | copy-start | bytes 1572868
  241.2 0.8 copy-start.3
  245.4 30.5 %all-to-all-start.3 = ((bf16[4,256,1024]{1,2,0:T(8,128)(2,1)}), bf16[4,256,1024]{1,2,0:T(8,128)(2,1)S(1)}, u32[]{:S(2)}, u32[]{:S(2)}) async-start(bf16[4,256,1024]{1,2,0:T(8,128)(2,1)} %broadcast_in_dim.17), calls=%async_computation.3 | async-start | bytes 4194304 | tf_op jit(solution)/shard_map/all_to_all | solution.py:29
  276.5 1.6 copy-start.5
  278.1 1.6 copy-start.4
  280.4 2.7 collective-permute-start.2
  281.8 3.1 collective-permute-start.3
  286.1 21.3 %copy-start = (bf16[1,64,16,1024]{3,2,0,1:T(8,128)(2,1)S(1)}, bf16[1,64,16,1024]{3,2,0,1:T(8,128)(2,1)}, u32[]{:S(2)}) copy-start(bf16[1,64,16,1024]{3,2,0,1:T(8,128)(2,1)} %get-tuple-element.16) | copy-start | bytes 6291460
  307.3 8.6 %copy-start.8 = (f32[1024]{0:T(1024)S(1)}, f32[1024]{0:T(1024)}, u32[]{:S(2)}) copy-start(f32[1024]{0:T(1024)} %param.15) | copy-start | bytes 12292
Sparse Core Ops, SparseCore 0:
  10.1 170.9 all-gather.2
where the time goes:
time: 325 us; the launch traced here: 324 us
  waiting for transfers between devices  201 us (62%)
  local copies, waits for them, and re-layouts  44.3 us (14%)
  blocking collectives  28.5 us (9%)
  starting transfers between devices  22.4 us (7%)
  between operations  13.7 us (4%)
  other arithmetic  8.1 us (2%)
  matrix products  5.66 us (2%)
    all_gather x1, waiting for transfers between devices, one_gather(): lines, at, finished = (lax.all_gather(ravelled, axis), 0, [])  135 us
    all_to_all x4, waiting for transfers between devices, copy_for_each(): lax.all_to_all(jnp.broadcast_to(value[None], (size, *value.shape)), axis,...  62.5 us
    all_to_all x3, blocking collectives, copy_for_each(): lax.all_to_all(jnp.broadcast_to(value[None], (size, *value.shape)), axis,...  28.5 us
    all_to_all x4, starting transfers between devices, copy_for_each(): lax.all_to_all(jnp.broadcast_to(value[None], (size, *value.shape)), axis,...  16.3 us
    all_gather x1, local copies, waits for them, and re-layouts, one_gather(): lines, at, finished = (lax.all_gather(ravelled, axis), 0, [])  13.5 us
    unnamed x27, local copies, waits for them, and re-layouts  13.5 us
    slice x1, local copies, waits for them, and re-layouts, one_gather(): pieces = lines[:, at:at + a.size].reshape(-1, *a.shape)  7.03 us
  transfers between devices with their start and end apart: 9, of which 7 were waited for; matrix products, arithmetic and copies ran while one was open for 4% of the time, Pallas kernels for 0%

commit v1 on v0

v1 whole, which is shorter than its diff:
```python
import jax
import jax.numpy as jnp
from jax import lax
from jax.sharding import PartitionSpec as P

LAYERS = 2
IN_SCALE = 2.0**19
OUT_SCALE = 2.0**17
X_SCALE = 2.0**6


def exchanged(value, axis):
    size = lax.axis_size(axis)
    return lax.all_to_all(
        jnp.broadcast_to(value[None], (size, *value.shape)), axis, 0, 0, tiled=True
    )


def joined(pieces):
    size, rows, width = pieces.shape
    return jnp.moveaxis(pieces, 0, 1).reshape(rows, size * width)


def with_neighbours(block, axis, width):
    count = lax.axis_size(axis)
    forward = [(i, i + 1) for i in range(count - 1)]
    backward = [(i + 1, i) for i in range(count - 1)]
    low = lax.ppermute(block[block.shape[0] - width :], axis, forward)
    high = lax.ppermute(block[:width], axis, backward)
    return jnp.concatenate([low, block, high], axis=0)


def packed(value, gate, out):
    width = value.shape[1] + gate.shape[1]
    projections = jnp.concatenate([value, gate], axis=1).astype(jnp.float32) * IN_SCALE
    out = out.astype(jnp.float32) * OUT_SCALE
    halves = [out[:, i : i + width] for i in range(0, out.shape[1], width)]
    return [projections.astype(jnp.float16)] + [h.astype(jnp.float16) for h in halves]


def unpacked(gathered, rows):
    parts, _, width = gathered.shape
    return gathered[:, rows].astype(jnp.bfloat16).reshape(-1, width)


def split_in_three(value):
    parts = []
    for _ in range(3):
        part = lax.reduce_precision(value, 8, 7)
        parts.append(part.astype(jnp.bfloat16))
        value = value - part
    return parts


def convolved(xf, projections, gain, taps, rows):
    scale = lax.rsqrt(jnp.mean(xf * xf, axis=1, keepdims=True) + 1e-06)
    normed = (xf * scale * gain[None, :]).astype(jnp.bfloat16)
    both = jnp.dot(normed, projections, preferred_element_type=jnp.float32) * (1 / IN_SCALE)
    half = both.shape[1] // 2
    value, gate = both[:, :half], both[:, half:]
    glu = (value * jax.nn.sigmoid(gate)).astype(jnp.bfloat16).astype(jnp.float32)
    reach = taps.shape[0] // 2
    first = (glu.shape[0] - rows) // 2 - reach
    conv = jnp.zeros((rows, half), jnp.float32)
    for tap in range(taps.shape[0]):
        conv = conv + taps[tap][None, :] * glu[first + tap : first + tap + rows]
    return conv.astype(jnp.bfloat16)


def projected(conv, gain, outs):
    conv = conv.astype(jnp.float32)
    center = jnp.mean(conv, axis=1, keepdims=True)
    shifted = conv - center
    spread = jnp.mean(shifted * shifted, axis=1, keepdims=True)
    act = jax.nn.silu(shifted * lax.rsqrt(spread + 1e-05) * gain[None, :]).astype(jnp.bfloat16)
    branch = [jnp.dot(act, o, preferred_element_type=jnp.float32) * (1 / OUT_SCALE) for o in outs]
    return jnp.concatenate(branch, axis=1)


def on_device(
    tokens, norm_gain, value_weight, gate_weight, conv_taps, channel_gain, out_weight, final_gain
):
    rows = tokens.shape[0]
    margin = 16
    x_local = with_neighbours(tokens, "sp", 2 * margin)
    coded = jnp.stack(split_in_three(channel_gain)).reshape(-1)
    width = tokens.shape[1]
    coded = jnp.pad(coded, (0, 2 * width - coded.shape[0])).reshape(2, width)
    sent = jnp.concatenate([coded[:1], x_local[1:-1], coded[1:]], axis=0)
    everyone = exchanged(sent, "tp")
    x_all = joined(everyone)
    gains = jnp.concatenate([everyone[:, 0], everyone[:, -1]], axis=1)[:, : 3 * channel_gain.size]
    gains = gains.reshape(-1, 3, *channel_gain.shape).astype(jnp.float32)
    gains = gains[:, 0] + (gains[:, 1] + gains[:, 2])
    gains = jnp.moveaxis(gains, 0, 1).reshape(LAYERS, -1)
    pieces = []
    for l in range(LAYERS):
        pieces += packed(value_weight[l], gate_weight[l], out_weight[l])
    weights = lax.all_gather(jnp.concatenate(pieces, axis=0), "sp")
    starts, at = [], 0
    for piece in pieces:
        starts.append(slice(at, at + piece.shape[0]))
        at += piece.shape[0]
    per = len(pieces) // LAYERS

    middle = rows + 2 * margin
    projections = unpacked(weights, starts[0])
    conv = convolved(
        x_all.astype(jnp.float32), projections, norm_gain[0], conv_taps[0], middle
    )
    conv, weights = lax.optimization_barrier((conv, weights))
    conv_all = joined(exchanged(conv, "tp"))
    outs = [unpacked(weights, s) for s in starts[1:per]]
    projections = unpacked(weights, starts[per])
    branch = projected(conv_all, gains[0], outs)
    position = lax.axis_index("sp") * rows - margin + lax.iota(jnp.int32, middle)
    inside = (position >= 0) & (position < rows * lax.axis_size("sp"))
    x_next = x_local[margin : margin + middle].astype(jnp.float32) + branch
    x_next = jnp.where(inside[:, None], x_next, 0.0).astype(jnp.bfloat16)

    shared = (x_next.astype(jnp.float32) * X_SCALE).astype(jnp.float16)
    x_all = joined(lax.all_gather(shared, "tp")).astype(jnp.float32) * (1 / X_SCALE)
    conv = convolved(x_all, projections, norm_gain[1], conv_taps[1], rows)
    conv, weights = lax.optimization_barrier((conv, weights))
    conv_all = joined(exchanged(conv, "tp"))
    outs = [unpacked(weights, s) for s in starts[per + 1 :]]
    branch = projected(conv_all, gains[1], outs)
    x_last = (x_next[margin : margin + rows].astype(jnp.float32) + branch).astype(jnp.bfloat16)

    xf = x_last.astype(jnp.float32)
    squares = jnp.sum(exchanged(jnp.sum(xf * xf, axis=1), "tp"), axis=0)
    width = xf.shape[1] * lax.axis_size("tp")
    scale = lax.rsqrt(squares / width + 1e-06)[:, None]
    return (xf * scale * final_gain[None, :]).astype(jnp.bfloat16)


def solution(mesh):
    placed = (
        P(("grp", "sp"), "tp"),
        P(),
        P(None, "sp", "tp"),
        P(None, "sp", "tp"),
        P(None, None, "tp"),
        P(None, "tp"),
        P(None, "sp", "tp"),
        P("tp"),
    )
    return jax.shard_map(
        on_device, mesh=mesh, in_specs=placed, out_specs=P(("grp", "sp"), "tp"), check_vma=False
    )
```

time: 325 us -> 257 us (0.79)
  waiting for transfers between devices: 201 us -> 9.14 us
  blocking collectives: 28.5 us -> 175 us
  local copies, waits for them, and re-layouts: 44.3 us -> 16 us
  other arithmetic: 8.1 us -> 29.6 us
  between operations: 13.7 us -> 0.6 us
  starting transfers between devices: 22.4 us -> 18.2 us
    all_gather x0 -> x2, blocking collectives: none -> 167 us  [the longest x1 145 us: on_device(): weights = lax.all_gather(jnp.concatenate(pieces, axis=0), 'sp')]
    all_gather x1 -> x0, waiting for transfers between devices: 135 us -> none  [one_gather(): lines, at, finished = (lax.all_gather(ravelled, axis), 0, [])]
    all_to_all x4 -> x3, waiting for transfers between devices: 62.5 us -> 9.13 us  [exchanged(): lax.all_to_all(jnp.broadcast_to(value[None], (size, *value.shape)), axis,...]
    all_to_all x3 -> x1, blocking collectives: 28.5 us -> 7.67 us  [exchanged(): lax.all_to_all(jnp.broadcast_to(value[None], (size, *value.shape)), axis,...]
    convert_element_type x6 -> x13, other arithmetic: 2.85 us -> 22.3 us  [the longest x4 15.2 us: unpacked(): return gathered[:, rows].astype(jnp.bfloat16).reshape(-1, width)]
    all_gather x1 -> x0, local copies, waits for them, and re-layouts: 13.5 us -> none  [one_gather(): lines, at, finished = (lax.all_gather(ravelled, axis), 0, [])]
    unnamed x27 -> x42, local copies, waits for them, and re-layouts: 13.5 us -> 3.36 us
    slice x12, local copies, waits for them, and re-layouts: 12.4 us -> 6.22 us  [the longest x4 5.04 us: convolved(): conv = conv + taps[tap][None, :] * glu[first + tap:first + tap + rows]]
  transfers between devices with their start and end apart: 9 -> 5, of which waited for: 7 -> 2; matrix products, arithmetic and copies ran while one was open for 4% -> 10% of each run, Pallas kernels for 0% -> 0%
where the time goes in v1:
time: 257 us; the launch traced here: 256 us
  blocking collectives  175 us (68%)
  other arithmetic  29.6 us (12%)
  starting transfers between devices  18.2 us (7%)
  local copies, waits for them, and re-layouts  16 us (6%)
  waiting for transfers between devices  9.14 us (4%)
  matrix products  7.73 us (3%)
    all_gather x1, blocking collectives, on_device(): weights = lax.all_gather(jnp.concatenate(pieces, axis=0), 'sp')  145 us
    all_gather x1, blocking collectives, on_device(): lax.all_gather(shared, 'tp')  22.8 us
    convert_element_type x4, other arithmetic, unpacked(): return gathered[:, rows].astype(jnp.bfloat16).reshape(-1, width)  15.2 us
    all_to_all x3, starting transfers between devices, exchanged(): lax.all_to_all(jnp.broadcast_to(value[None], (size, *value.shape)), axis,...  13.8 us
    all_to_all x3, waiting for transfers between devices, exchanged(): lax.all_to_all(jnp.broadcast_to(value[None], (size, *value.shape)), axis,...  9.13 us
    all_to_all x1, blocking collectives, exchanged(): lax.all_to_all(jnp.broadcast_to(value[None], (size, *value.shape)), axis,...  7.67 us
    dot_general x2, matrix products, convolved(): jnp.dot(normed, projections, preferred_element_type=jnp.float32)  5.88 us
  transfers between devices with their start and end apart: 5, of which 2 were waited for; matrix products, arithmetic and copies ran while one was open for 10% of the time, Pallas kernels for 0%

profile of v1, /device:TPU:40, one launch (start us, length us, event | category | flops | bytes accessed | tf_op | source)
XLA Modules:
  0.0 256.3 jit_solution(12486225389117514934)
XLA Ops:
  0.0 0.9 fusion.127
  0.9 1.3 collective-permute-start.1
  2.2 3.1 %collective-permute-start = (bf16[32,1024]{1,0:T(8,128)(2,1)S(1)}, bf16[32,1024]{1,0:T(8,128)(2,1)S(1)}, u32[]{:S(2)}, u32[]{:S(2)}) collective-permute-start(bf16[32,1024]{1,0:T(8,128)(2,1)S(1)} %get-tuple-element.26), channel_id=1, source_target_pairs={{0,4},{4,8},{8,12},{12,16},{16,20},{20,24},{24,28},{28,32},{32,36}... | collective-permute-start | bytes 196616 | tf_op jit(solution)/shard_map/ppermute | solution.py:28
  5.3 0.7 fusion.121
  6.0 0.8 fusion.112
  6.8 0.8 slice_bitcast_fusion
  7.8 1.1 constant_dynamic-update-slice_fusion.1
  9.3 1.8 broadcast_in_dim.21
  11.1 4.6 %all-to-all-start = ((bf16[4,320,1024]{2,1,0:T(8,128)(2,1)}), bf16[4,320,1024]{2,1,0:T(8,128)(2,1)S(1)}, u32[]{:S(2)}, u32[]{:S(2)}) async-start(bf16[4,320,1024]{2,1,0:T(8,128)(2,1)} %broadcast_in_dim.21), calls=%async_computation | async-start | bytes 5242880 | tf_op jit(solution)/shard_map/all_to_all | solution.py:14
  15.7 144.5 %all-gather.4 = f16[12288,512]{1,0:T(8,128)(2,1)} all-gather(f16[192,512]{1,0:T(8,128)(2,1)S(1)} %constant_dynamic-update-slice_fusion.3), channel_id=2, replica_groups=mesh['grp'=2,'sp'=64,'tp'=4] {'sp'}, dimensions={0}, use_global_device_ids=true | all-gather | bytes 12779520 | tf_op jit(solution)/shard_map/all_gather | solution.py:99
  160.3 0.6 fusion.120
  160.9 0.8 fusion.131
  161.7 1.4 fusion.128
  163.1 1.5 fusion.129
  164.6 1.4 fusion.130
  166.0 5.5 %slice_convert_fusion = bf16[64,64,512]{2,1,0:T(8,128)(2,1)} fusion(f16[64,192,512]{2,1,0:T(8,128)(2,1)} %bitcast.162), kind=kLoop, calls=%fused_computation.9 | loop fusion | flops 2097152 | bytes 8388608 | tf_op jit(solution)/shard_map/convert_element_type | solution.py:43
  171.4 0.6 fusion
  172.1 1.0 fusion.5
  173.0 1.9 copy.33
  175.0 4.5 %convolution_multiply_fusion = f32[320,512]{1,0:T(8,128)S(1)} fusion(bf16[320,4096]{1,0:T(8,128)(2,1)} %bitcast.175, bf16[4096,512]{1,0:T(8,128)(2,1)} %bitcast.172), kind=kOutput, calls=%fused_computation.20 | convolution fusion | flops 1342341120 | bytes 7471104 | tf_op jit(solution)/shard_map/dot_general | solution.py:58
  179.6 0.8 fusion.45
  180.4 0.9 broadcast_in_dim.22
  181.2 5.7 %all-to-all-start.1 = ((bf16[4,288,256]{2,1,0:T(8,128)(2,1)}), bf16[4,288,256]{2,1,0:T(8,128)(2,1)S(1)}, u32[]{:S(2)}, u32[]{:S(2)}) async-start(bf16[4,288,256]{2,1,0:T(8,128)(2,1)} %broadcast_in_dim.22), calls=%async_computation.1 | async-start | bytes 1179648 | tf_op jit(solution)/shard_map/all_to_all | solution.py:14
  186.9 2.1 slice_convert_fusion.5
  189.1 5.5 %slice_convert_fusion.1 = bf16[64,64,512]{2,1,0:T(8,128)(2,1)} fusion(f16[64,192,512]{2,1,0:T(8,128)(2,1)} %bitcast.164), kind=kLoop, calls=%fused_computation.10 | loop fusion | flops 2097152 | bytes 8388608 | tf_op jit(solution)/shard_map/convert_element_type | solution.py:43
  194.5 3.1 %all-to-all-done.1 = bf16[4,288,256]{2,1,0:T(8,128)(2,1)S(1)} async-done(((bf16[4,288,256]{2,1,0:T(8,128)(2,1)}), bf16[4,288,256]{2,1,0:T(8,128)(2,1)S(1)}, u32[]{:S(2)}, u32[]{:S(2)}) %all-to-all-start.1) | async-done | bytes 589856 | tf_op jit(solution)/shard_map/all_to_all | solution.py:14
  197.8 0.3 fusion.10
  198.1 0.5 fusion.34
  198.7 0.5 convolution_multiply_fusion.3
  199.2 0.5 convolution_multiply_fusion.2
  199.7 1.1 multiply_convert_fusion
  200.8 22.8 %all-gather.5 = f16[1152,1024]{1,0:T(8,128)(2,1)S(1)} all-gather(f16[288,1024]{1,0:T(8,128)(2,1)S(1)} %get-tuple-element.17), channel_id=3, replica_groups=mesh['grp'=2,'sp'=64,'tp'=4] {'tp'}, dimensions={0}, use_global_device_ids=true | all-gather | bytes 2949120 | tf_op jit(solution)/shard_map/all_gather | solution.py:122
  223.6 0.7 multiply_reduce_fusion
  224.3 0.6 convert.13
  224.9 3.4 %fusion.4 = bf16[4,288,1024]{2,0,1:T(4,128)(2,1)S(1)} fusion(f32[4,288,1024]{2,1,0:T(8,128)S(1)} %convert.13, f32[4,1024]{1,0:T(4,128)S(1)} %mul.966, f32[288]{0:T(512)S(1)} %rsqrt_multiply_fusion), kind=kLoop, calls=%fused_computation.7 | loop fusion | flops 3538944 | bytes 7095424 | tf_op jit(solution)/shard_map/convert_element_type | solution.py:57
  228.3 1.0 copy.36
  229.4 1.2 copy-done
  230.6 1.4 convolution_multiply_fusion.1
  232.2 0.7 fusion.77
  233.0 0.8 broadcast_in_dim.24
  233.8 3.6 %all-to-all-start.2 = ((bf16[4,256,256]{1,2,0:T(8,128)(2,1)}), bf16[4,256,256]{1,2,0:T(8,128)(2,1)S(1)}, u32[]{:S(2)}, u32[]{:S(2)}) async-start(bf16[4,256,256]{1,2,0:T(8,128)(2,1)} %broadcast_in_dim.24), calls=%async_computation.2 | async-start | bytes 1048576 | tf_op jit(solution)/shard_map/all_to_all | solution.py:14
  237.4 2.1 slice_convert_fusion.3
  239.6 6.0 %all-to-all-done.2 = bf16[4,256,256]{1,2,0:T(8,128)(2,1)S(1)} async-done(((bf16[4,256,256]{1,2,0:T(8,128)(2,1)}), bf16[4,256,256]{1,2,0:T(8,128)(2,1)S(1)}, u32[]{:S(2)}, u32[]{:S(2)}) %all-to-all-start.2) | async-done | bytes 524320 | tf_op jit(solution)/shard_map/all_to_all | solution.py:14
  246.0 0.4 fusion.29
  246.4 0.5 convolution_multiply_fusion.5
  246.9 0.5 convolution_multiply_fusion.4
  247.6 7.7 %all_to_all.21 = f32[4,1,256]{2,1,0:T(1,128)S(1)} all-to-all(f32[4,1,256]{2,1,0:T(1,128)S(1)} %broadcast_in_dim.25), channel_id=1, replica_groups=mesh['grp'=2,'sp'=64,'tp'=4] {'tp'}, dimensions={0} | all-to-all | bytes 8192 | tf_op jit(solution)/shard_map/all_to_all | solution.py:14
  255.3 1.0 fusion.32
  (80 shorter events, 2.0 us)
Async XLA Ops:
  0.9 8.0 %collective-permute-start.1 = (bf16[32,1024]{1,0:T(8,128)(2,1)S(1)}, bf16[32,1024]{1,0:T(8,128)(2,1)S(1)}, u32[]{:S(2)}, u32[]{:S(2)}) collective-permute-start(bf16[32,1024]{1,0:T(8,128)(2,1)S(1)} %get-tuple-element.25), channel_id=1, source_target_pairs={{4,0},{8,4},{12,8},{16,12},{20,16},{24,20},{28,24},{32,28},{36,32}... | collective-permute-start | bytes 196616 | tf_op jit(solution)/shard_map/ppermute | solution.py:29
  2.2 5.6 %collective-permute-start = (bf16[32,1024]{1,0:T(8,128)(2,1)S(1)}, bf16[32,1024]{1,0:T(8,128)(2,1)S(1)}, u32[]{:S(2)}, u32[]{:S(2)}) collective-permute-start(bf16[32,1024]{1,0:T(8,128)(2,1)S(1)} %get-tuple-element.26), channel_id=1, source_target_pairs={{0,4},{4,8},{8,12},{12,16},{16,20},{20,24},{24,28},{28,32},{32,36}... | collective-permute-start | bytes 196616 | tf_op jit(solution)/shard_map/ppermute | solution.py:28
  11.1 160.3 %all-to-all-start = ((bf16[4,320,1024]{2,1,0:T(8,128)(2,1)}), bf16[4,320,1024]{2,1,0:T(8,128)(2,1)S(1)}, u32[]{:S(2)}, u32[]{:S(2)}) async-start(bf16[4,320,1024]{2,1,0:T(8,128)(2,1)} %broadcast_in_dim.21), calls=%async_computation | async-start | bytes 5242880 | tf_op jit(solution)/shard_map/all_to_all | solution.py:14
  15.7 144.5 %copy-start.2 = (f32[2,4096]{1,0:T(2,128)S(1)}, f32[2,4096]{1,0:T(2,128)}, u32[]{:S(2)}) copy-start(f32[2,4096]{1,0:T(2,128)} %param.9) | copy-start | bytes 98308
  181.2 16.4 %all-to-all-start.1 = ((bf16[4,288,256]{2,1,0:T(8,128)(2,1)}), bf16[4,288,256]{2,1,0:T(8,128)(2,1)S(1)}, u32[]{:S(2)}, u32[]{:S(2)}) async-start(bf16[4,288,256]{2,1,0:T(8,128)(2,1)} %broadcast_in_dim.22), calls=%async_computation.1 | async-start | bytes 1179648 | tf_op jit(solution)/shard_map/all_to_all | solution.py:14
  198.6 1.0 copy-start.16
  228.3 2.2 copy-start
  230.5 1.6 copy-start.4
  230.5 1.6 copy-start.5
  230.5 1.6 copy-start.6
  230.5 1.6 copy-start.7
  230.5 1.6 copy-start.8
  230.5 1.6 copy-start.9
  230.6 1.6 copy-start.10
  230.6 1.6 copy-start.11
  230.6 1.6 copy-start.12
  230.6 1.6 copy-start.13
  230.6 1.6 copy-start.14
  230.6 1.6 copy-start.15
  233.8 11.8 %all-to-all-start.2 = ((bf16[4,256,256]{1,2,0:T(8,128)(2,1)}), bf16[4,256,256]{1,2,0:T(8,128)(2,1)S(1)}, u32[]{:S(2)}, u32[]{:S(2)}) async-start(bf16[4,256,256]{1,2,0:T(8,128)(2,1)} %broadcast_in_dim.24), calls=%async_computation.2 | async-start | bytes 1048576 | tf_op jit(solution)/shard_map/all_to_all | solution.py:14
  246.0 1.3 copy-start.1
  246.8 8.4 %copy-start.3 = (f32[1024]{0:T(1024)S(1)}, f32[1024]{0:T(1024)}, u32[]{:S(2)}) copy-start(f32[1024]{0:T(1024)} %param.15) | copy-start | bytes 12292

commit v2 on v1

--- a/solution.py
+++ b/solution.py
@@ -1,6 +1,10 @@
+import functools
+
 import jax
 import jax.numpy as jnp
 from jax import lax
+from jax.experimental import pallas as pl
+from jax.experimental.pallas import tpu as pltpu
 from jax.sharding import PartitionSpec as P
 
 LAYERS = 2
@@ -21,13 +25,13 @@
     return jnp.moveaxis(pieces, 0, 1).reshape(rows, size * width)
 
 
-def with_neighbours(block, axis, width):
+def neighbours(block, axis, width):
     count = lax.axis_size(axis)
     forward = [(i, i + 1) for i in range(count - 1)]
     backward = [(i + 1, i) for i in range(count - 1)]
     low = lax.ppermute(block[block.shape[0] - width :], axis, forward)
     high = lax.ppermute(block[:width], axis, backward)
-    return jnp.concatenate([low, block, high], axis=0)
+    return low, high
 
 
 def packed(value, gate, out):
@@ -52,19 +56,77 @@
     return parts
 
 
-def convolved(xf, projections, gain, taps, rows):
-    scale = lax.rsqrt(jnp.mean(xf * xf, axis=1, keepdims=True) + 1e-06)
-    normed = (xf * scale * gain[None, :]).astype(jnp.bfloat16)
-    both = jnp.dot(normed, projections, preferred_element_type=jnp.float32) * (1 / IN_SCALE)
-    half = both.shape[1] // 2
-    value, gate = both[:, :half], both[:, half:]
-    glu = (value * jax.nn.sigmoid(gate)).astype(jnp.bfloat16).astype(jnp.float32)
-    reach = taps.shape[0] // 2
-    first = (glu.shape[0] - rows) // 2 - reach
-    conv = jnp.zeros((rows, half), jnp.float32)
-    for tap in range(taps.shape[0]):
-        conv = conv + taps[tap][None, :] * glu[first + tap : first + tap + rows]
-    return conv.astype(jnp.bfloat16)
+def convolved_kernel(first, x_ref, w_ref, gain_ref, taps_ref, out_ref, scaled_ref, glu_ref):
+    pieces, rows_in, width = x_ref.shape
+    count, rows, half = out_ref.shape
+    block = 32
+    blocks = range(0, rows_in, block)
+
+    squares = [jnp.zeros((block, 128), jnp.float32) for _ in blocks]
+    both = None
+    for j in range(pieces):
+        for i, at in enumerate(blocks):
+            for b in range(0, width, 128):
+                xf = x_ref[j, at : at + block, b : b + 128].astype(jnp.float32)
+                squares[i] = squares[i] + xf * xf
+                scaled = (xf * gain_ref[j, :, b : b + 128]).astype(jnp.bfloat16)
+                scaled_ref[j, at : at + block, b : b + 128] = scaled
+        part = jnp.dot(scaled_ref[j], w_ref[j], preferred_element_type=jnp.float32)
+        both = part if both is None else both + part
+    for i, at in enumerate(blocks):
+        mean = jnp.sum(squares[i], axis=1, keepdims=True) / (pieces * width)
+        scale = lax.rsqrt(mean + 1e-06) * (1 / IN_SCALE)
+        value = both[at : at + block, :half] * scale
+        gate = both[at : at + block, half:] * scale
+        glu = (value * jax.nn.sigmoid(gate)).astype(jnp.bfloat16)
+        glu_ref[0, at : at + block, :] = glu.astype(jnp.float32)
+    reach_rows = rows_in - 8
+    for shift in range(1, 8):
+        glu_ref[shift, :reach_rows, :] = glu_ref[0, shift : shift + reach_rows, :]
+
+    def convolve(i, carry):
+        base = pl.multiple_of(i * block, block)
+        for lane in range(0, half, 128):
+            lanes = slice(lane, lane + 128)
+            conv = jnp.zeros((block, 128), jnp.float32)
+            for tap in range(taps_ref.shape[0]):
+                down, shift = divmod(first + tap, 8)
+                moved = glu_ref[shift, pl.ds(pl.multiple_of(base + 8 * down, 8), block), lanes]
+                conv = conv + taps_ref[tap : tap + 1, lanes] * moved
+            conv = conv.astype(jnp.bfloat16)
+            for c in range(count):
+                out_ref[c, pl.ds(base, block), lanes] = conv
+        return carry
+
+    lax.fori_loop(0, rows // block, convolve, 0)
+
+
+def convolved(pieces, projections, gain, taps, rows):
+    count, rows_in, width = pieces.shape
+    both = projections.shape[1]
+    half = both // 2
+    first = (rows_in - rows) // 2 - taps.shape[0] // 2
+    vmem = pl.BlockSpec(memory_space=pltpu.VMEM)
+    return pl.pallas_call(
+        functools.partial(convolved_kernel, first),
+        out_shape=jax.ShapeDtypeStruct((count, rows, half), jnp.bfloat16),
+        in_specs=[vmem] * 4,
+        out_specs=vmem,
+        scratch_shapes=[
+            pltpu.VMEM((count, rows_in, width), jnp.bfloat16),
+            pltpu.VMEM((8, rows_in, half), jnp.float32),
+        ],
+        cost_estimate=pl.CostEstimate(
+            flops=2 * rows_in * count * width * both,
+            bytes_accessed=2 * (count * width * both + count * rows_in * width),
+            transcendentals=rows_in * half,
+        ),
+    )(
+        pieces,
+        projections.reshape(count, width, both),
+        gain.reshape(count, 1, width),
+        taps,
+    )
 
 
 def projected(conv, gain, outs):
@@ -82,13 +144,13 @@
 ):
     rows = tokens.shape[0]
     margin = 16
-    x_local = with_neighbours(tokens, "sp", 2 * margin)
+    low, high = neighbours(tokens, "sp", 2 * margin)
     coded = jnp.stack(split_in_three(channel_gain)).reshape(-1)
     width = tokens.shape[1]
     coded = jnp.pad(coded, (0, 2 * width - coded.shape[0])).reshape(2, width)
-    sent = jnp.concatenate([coded[:1], x_local[1:-1], coded[1:]], axis=0)
-    everyone = exchanged(sent, "tp")
-    x_all = joined(everyone)
+    x_local = jnp.concatenate([low, tokens, high], axis=0)
+    everyone = exchanged(jnp.concatenate([coded[:1], x_local[1:-1], coded[1:]], axis=0), "tp")
+    x_local = x_local[margin:-margin]
     gains = jnp.concatenate([everyone[:, 0], everyone[:, -1]], axis=1)[:, : 3 * channel_gain.size]
     gains = gains.reshape(-1, 3, *channel_gain.shape).astype(jnp.float32)
     gains = gains[:, 0] + (gains[:, 1] + gains[:, 2])
@@ -105,24 +167,22 @@
 
     middle = rows + 2 * margin
     projections = unpacked(weights, starts[0])
-    conv = convolved(
-        x_all.astype(jnp.float32), projections, norm_gain[0], conv_taps[0], middle
-    )
+    conv = convolved(everyone, projections, norm_gain[0], conv_taps[0], middle)
     conv, weights = lax.optimization_barrier((conv, weights))
-    conv_all = joined(exchanged(conv, "tp"))
+    conv_all = joined(lax.all_to_all(conv, "tp", 0, 0, tiled=True))
     outs = [unpacked(weights, s) for s in starts[1:per]]
     projections = unpacked(weights, starts[per])
     branch = projected(conv_all, gains[0], outs)
     position = lax.axis_index("sp") * rows - margin + lax.iota(jnp.int32, middle)
     inside = (position >= 0) & (position < rows * lax.axis_size("sp"))
-    x_next = x_local[margin : margin + middle].astype(jnp.float32) + branch
+    x_next = x_local.astype(jnp.float32) + branch
     x_next = jnp.where(inside[:, None], x_next, 0.0).astype(jnp.bfloat16)
 
     shared = (x_next.astype(jnp.float32) * X_SCALE).astype(jnp.float16)
-    x_all = joined(lax.all_gather(shared, "tp")).astype(jnp.float32) * (1 / X_SCALE)
-    conv = convolved(x_all, projections, norm_gain[1], conv_taps[1], rows)
+    x_all = lax.all_gather(shared, "tp").astype(jnp.float32) * (1 / X_SCALE)
+    conv = convolved(x_all.astype(jnp.bfloat16), projections, norm_gain[1], conv_taps[1], rows)
     conv, weights = lax.optimization_barrier((conv, weights))
-    conv_all = joined(exchanged(conv, "tp"))
+    conv_all = joined(lax.all_to_all(conv, "tp", 0, 0, tiled=True))
     outs = [unpacked(weights, s) for s in starts[per + 1 :]]
     branch = projected(conv_all, gains[1], outs)
     x_last = (x_next[margin : margin + rows].astype(jnp.float32) + branch).astype(jnp.bfloat16)

time: 257 us -> 250 us (0.973)
  Pallas kernels: 0 us -> 13.5 us
  local copies, waits for them, and re-layouts: 16 us -> 8.51 us
  other arithmetic: 29.6 us -> 23.6 us
  matrix products: 7.73 us -> 3.07 us
  starting transfers between devices: 18.2 us -> 15.3 us
    pallas_call x0 -> x2, Pallas kernels: none -> 13.5 us  [convolved(): pl.pallas_call(functools.partial(convolved_kernel, first), out_shape=jax....]
    all_to_all x3 -> x1, starting transfers between devices: 13.8 us -> 4.58 us  [exchanged(): lax.all_to_all(jnp.broadcast_to(value[None], (size, *value.shape)), axis,...]
    all_to_all x3 -> x1, waiting for transfers between devices: 9.13 us -> 0.01 us  [exchanged(): lax.all_to_all(jnp.broadcast_to(value[None], (size, *value.shape)), axis,...]
    all_to_all x0 -> x2, starting transfers between devices: none -> 7.6 us  [on_device(): conv_all = joined(lax.all_to_all(conv, 'tp', 0, 0, tiled=True))]
    all_to_all x0 -> x2, waiting for transfers between devices: none -> 7.14 us  [on_device(): conv_all = joined(lax.all_to_all(conv, 'tp', 0, 0, tiled=True))]
    dot_general x2 -> x0, matrix products: 5.88 us -> none  [convolved(): jnp.dot(normed, projections, preferred_element_type=jnp.float32)]
    slice x11 -> x7, local copies, waits for them, and re-layouts: 6.19 us -> 1.81 us  [the longest x1 0.94 us: neighbours(): high = lax.ppermute(block[:width], axis, backward)]
    convert_element_type x6 -> x1, other arithmetic: 5.65 us -> 2.1 us  [on_device(): x_all.astype(jnp.bfloat16)]
  transfers between devices with their start and end apart: 5 -> 5, of which waited for: 2 -> 3; matrix products, arithmetic and copies ran while one was open for 10% -> 9% of each run, Pallas kernels for 0% -> 0%
where the time goes in v2:
time: 250 us; the launch traced here: 249 us
  blocking collectives  176 us (70%)
  other arithmetic  23.6 us (9%)
  starting transfers between devices  15.3 us (6%)
  Pallas kernels  13.5 us (5%)
  waiting for transfers between devices  8.9 us (4%)
  local copies, waits for them, and re-layouts  8.51 us (3%)
  matrix products  3.07 us (1%)
    all_gather x1, blocking collectives, on_device(): weights = lax.all_gather(jnp.concatenate(pieces, axis=0), 'sp')  146 us
    all_gather x1, blocking collectives, on_device(): x_all = lax.all_gather(shared, 'tp').astype(jnp.float32) * (1 / X_SCALE)  22.9 us
    convert_element_type x4, other arithmetic, unpacked(): return gathered[:, rows].astype(jnp.bfloat16).reshape(-1, width)  16.3 us
    pallas_call x2, Pallas kernels, convolved(): pl.pallas_call(functools.partial(convolved_kernel, first), out_shape=jax....  13.5 us
    all_to_all x1, blocking collectives, exchanged(): lax.all_to_all(jnp.broadcast_to(value[None], (size, *value.shape)), axis,...  7.67 us
    all_to_all x2, starting transfers between devices, on_device(): conv_all = joined(lax.all_to_all(conv, 'tp', 0, 0, tiled=True))  7.6 us
    all_to_all x2, waiting for transfers between devices, on_device(): conv_all = joined(lax.all_to_all(conv, 'tp', 0, 0, tiled=True))  7.14 us
  transfers between devices with their start and end apart: 5, of which 3 were waited for; matrix products, arithmetic and copies ran while one was open for 9% of the time, Pallas kernels for 0%

profile of v2, /device:TPU:40, one launch (start us, length us, event | category | flops | bytes accessed | tf_op | source)
XLA Modules:
  0.0 249.2 jit_solution(2793562438144711656)
XLA Ops:
  0.0 0.9 fusion.46
  0.9 1.8 collective-permute-start
  2.8 1.3 collective-permute-start.1
  4.1 0.7 fusion.40
  4.9 0.8 fusion.32
  5.7 0.8 slice_bitcast_fusion
  6.7 1.8 collective-permute-done.1
  8.5 0.2 slice.155
  8.6 0.2 pad_maximum_fusion
  8.8 1.8 broadcast_in_dim.17
  10.7 4.6 %all-to-all-start = ((bf16[4,320,1024]{2,1,0:T(8,128)(2,1)}), bf16[4,320,1024]{2,1,0:T(8,128)(2,1)S(1)}, u32[]{:S(2)}, u32[]{:S(2)}) async-start(bf16[4,320,1024]{2,1,0:T(8,128)(2,1)} %broadcast_in_dim.17), calls=%async_computation | async-start | bytes 5242880 | tf_op jit(solution)/shard_map/all_to_all | solution.py:18
  15.2 145.5 %all-gather.4 = f16[12288,512]{1,0:T(8,128)(2,1)} all-gather(f16[192,512]{1,0:T(8,128)(2,1)S(1)} %constant_dynamic-update-slice_fusion.3), channel_id=2, replica_groups=mesh['grp'=2,'sp'=64,'tp'=4] {'sp'}, dimensions={0}, use_global_device_ids=true | all-gather | bytes 12779520 | tf_op jit(solution)/shard_map/all_gather | solution.py:161
  160.8 0.1 fusion.47
  160.8 0.6 copy.57
  161.5 0.6 copy.56
  162.1 5.5 %slice_convert_fusion = bf16[64,64,512]{2,1,0:T(8,128)(2,1)} fusion(f16[64,192,512]{2,1,0:T(8,128)(2,1)} %bitcast.98), kind=kLoop, calls=%fused_computation.1 | loop fusion | flops 2097152 | bytes 8388608 | tf_op jit(solution)/shard_map/convert_element_type | solution.py:47
  167.5 0.6 fusion.48
  168.2 0.0 all-to-all-done.x_ref
  168.2 1.5 copy-done
  169.7 6.9 %shard_map.82 = bf16[4,288,256]{2,1,0:T(8,128)(2,1)} custom-call(bf16[4,320,1024]{2,1,0:T(8,128)(2,1)} %copy-done, bf16[4,1024,512]{2,1,0:T(8,128)(2,1)} %bitcast.103, f32[4,1,1024]{2,1,0:T(1,128)} %bitcast.116, f32[31,256]{1,0:T(8,128)} %bitcast.114), custom_call_target="tpu_custom_call" | custom-call | flops 1342177280 | bytes 6815744 | tf_op jit(solution)/shard_map/pallas_call | solution.py:110
  176.7 4.0 %all-to-all-start.1 = ((bf16[4,288,256]{2,1,0:T(8,128)(2,1)}), bf16[4,288,256]{2,1,0:T(8,128)(2,1)S(1)}, u32[]{:S(2)}, u32[]{:S(2)}) async-start(bf16[4,288,256]{2,1,0:T(8,128)(2,1)} %shard_map.82), calls=%async_computation.1 | async-start | bytes 1179648 | tf_op jit(solution)/shard_map/all_to_all | solution.py:172
  180.7 0.9 fusion.45
  181.7 2.1 slice_convert_fusion.5
  183.8 5.5 %slice_convert_fusion.1 = bf16[64,64,512]{2,1,0:T(8,128)(2,1)} fusion(f16[64,192,512]{2,1,0:T(8,128)(2,1)} %bitcast.100), kind=kLoop, calls=%fused_computation.2 | loop fusion | flops 2097152 | bytes 8388608 | tf_op jit(solution)/shard_map/convert_element_type | solution.py:47
  189.3 2.1 all-to-all-done.1
  191.4 0.2 convert_reduce_fusion
  191.6 0.3 fusion.4
  191.9 0.5 fusion.28
  192.4 0.1 copy.49
  192.5 0.5 convolution_multiply_fusion
  193.0 0.5 convolution_multiply_fusion.1
  193.5 0.3 multiply_convert_fusion.1
  193.7 22.9 %all-gather.5 = f16[1152,1024]{1,0:T(8,128)(2,1)S(1)} all-gather(f16[288,1024]{1,0:T(8,128)(2,1)S(1)} %get-tuple-element.15), channel_id=3, replica_groups=mesh['grp'=2,'sp'=64,'tp'=4] {'tp'}, dimensions={0}, use_global_device_ids=true | all-gather | bytes 2949120 | tf_op jit(solution)/shard_map/all_gather | solution.py:182
  216.6 2.1 multiply_convert_fusion
  218.7 6.5 %shard_map.83 = bf16[4,256,256]{2,1,0:T(8,128)(2,1)} custom-call(bf16[4,288,1024]{2,1,0:T(8,128)(2,1)} %bitcast.104, bf16[4,1024,512]{2,1,0:T(8,128)(2,1)} %bitcast.102, f32[4,1,1024]{2,1,0:T(1,128)} %bitcast.115, f32[31,256]{1,0:T(8,128)} %bitcast.113), custom_call_target="tpu_custom_call" | custom-call | flops 1207959552 | bytes 6553600 | tf_op jit(solution)/shard_map/pallas_call | solution.py:110
  225.2 3.6 %all-to-all-start.2 = ((bf16[4,256,256]{2,1,0:T(8,128)(2,1)}), bf16[4,256,256]{2,1,0:T(8,128)(2,1)S(1)}, u32[]{:S(2)}, u32[]{:S(2)}) async-start(bf16[4,256,256]{2,1,0:T(8,128)(2,1)} %shard_map.83), calls=%async_computation.2 | async-start | bytes 1048576 | tf_op jit(solution)/shard_map/all_to_all | solution.py:185
  228.8 3.2 %slice_convert_fusion.3 = (bf16[64,16,512]{2,1,0:T(8,128)(2,1)S(1)}, bf16[64,16,512]{2,1,0:T(8,128)(2,1)}) fusion(f16[64,192,512]{2,1,0:T(8,128)(2,1)} %bitcast.101), kind=kLoop, calls=%fused_computation.45 | loop fusion | flops 1048576 | bytes 4194304 | tf_op jit(solution)/shard_map/convert_element_type | solution.py:47
  232.0 5.0 %all-to-all-done.2 = bf16[4,256,256]{2,1,0:T(8,128)(2,1)S(1)} async-done(((bf16[4,256,256]{2,1,0:T(8,128)(2,1)}), bf16[4,256,256]{2,1,0:T(8,128)(2,1)S(1)}, u32[]{:S(2)}, u32[]{:S(2)}) %all-to-all-start.2) | async-done | bytes 524320 | tf_op jit(solution)/shard_map/all_to_all | solution.py:185
  237.0 0.1 convert_reduce_fusion.1
  237.2 0.3 fusion.15
  237.5 0.5 fusion.23
  237.9 0.2 copy.42
  238.1 1.7 convolution_multiply_fusion.2
  239.8 0.5 convolution_multiply_fusion.3
  240.3 0.0 copy-start.4
  240.3 0.2 fusion.24
  240.5 7.7 %all_to_all.21 = f32[4,1,256]{2,1,0:T(1,128)S(1)} all-to-all(f32[4,1,256]{2,1,0:T(1,128)S(1)} %broadcast_in_dim.19), channel_id=1, replica_groups=mesh['grp'=2,'sp'=64,'tp'=4] {'tp'}, dimensions={0} | all-to-all | bytes 8192 | tf_op jit(solution)/shard_map/all_to_all | solution.py:18
  248.3 1.0 fusion.26
  (37 shorter events, 0.3 us)
Async XLA Ops:
  0.0 6.7 %copy-start.1 = (bf16[256,1024]{1,0:T(8,128)(2,1)S(1)}, bf16[256,1024]{1,0:T(8,128)(2,1)}, u32[]{:S(2)}) copy-start(bf16[256,1024]{1,0:T(8,128)(2,1)} %param.8) | copy-start | bytes 1572868
  0.9 5.7 %collective-permute-start = (bf16[32,1024]{1,0:T(8,128)(2,1)S(1)}, bf16[32,1024]{1,0:T(8,128)(2,1)S(1)}, u32[]{:S(2)}, u32[]{:S(2)}) collective-permute-start(bf16[32,1024]{1,0:T(8,128)(2,1)S(1)} %get-tuple-element.24), channel_id=1, source_target_pairs={{0,4},{4,8},{8,12},{12,16},{16,20},{20,24},{24,28},{28,32},{32,36}... | collective-permute-start | bytes 196616 | tf_op jit(solution)/shard_map/ppermute | solution.py:32
  2.8 5.7 %collective-permute-start.1 = (bf16[32,1024]{1,0:T(8,128)(2,1)S(1)}, bf16[32,1024]{1,0:T(8,128)(2,1)S(1)}, u32[]{:S(2)}, u32[]{:S(2)}) collective-permute-start(bf16[32,1024]{1,0:T(8,128)(2,1)S(1)} %get-tuple-element.23), channel_id=1, source_target_pairs={{4,0},{8,4},{12,8},{16,12},{20,16},{24,20},{28,24},{32,28},{36,32}... | collective-permute-start | bytes 196616 | tf_op jit(solution)/shard_map/ppermute | solution.py:33
  10.7 157.5 %all-to-all-start = ((bf16[4,320,1024]{2,1,0:T(8,128)(2,1)}), bf16[4,320,1024]{2,1,0:T(8,128)(2,1)S(1)}, u32[]{:S(2)}, u32[]{:S(2)}) async-start(bf16[4,320,1024]{2,1,0:T(8,128)(2,1)} %broadcast_in_dim.17), calls=%async_computation | async-start | bytes 5242880 | tf_op jit(solution)/shard_map/all_to_all | solution.py:18
  15.2 145.5 %copy-start.2 = (f32[2,31,256]{2,0,1:T(2,128)S(1)}, f32[2,31,256]{2,0,1:T(2,128)}, u32[]{:S(2)}) copy-start(f32[2,31,256]{2,0,1:T(2,128)} %param.12) | copy-start | bytes 190468
  162.1 5.5 %copy-start.3 = (f32[2,4096]{1,0:T(2,128)S(1)}, f32[2,4096]{1,0:T(2,128)}, u32[]{:S(2)}) copy-start(f32[2,4096]{1,0:T(2,128)} %param.9) | copy-start | bytes 98308
  168.2 1.5 copy-start
  176.7 14.8 %all-to-all-start.1 = ((bf16[4,288,256]{2,1,0:T(8,128)(2,1)}), bf16[4,288,256]{2,1,0:T(8,128)(2,1)S(1)}, u32[]{:S(2)}, u32[]{:S(2)}) async-start(bf16[4,288,256]{2,1,0:T(8,128)(2,1)} %shard_map.82), calls=%async_computation.1 | async-start | bytes 1179648 | tf_op jit(solution)/shard_map/all_to_all | solution.py:172
  225.2 11.8 %all-to-all-start.2 = ((bf16[4,256,256]{2,1,0:T(8,128)(2,1)}), bf16[4,256,256]{2,1,0:T(8,128)(2,1)S(1)}, u32[]{:S(2)}, u32[]{:S(2)}) async-start(bf16[4,256,256]{2,1,0:T(8,128)(2,1)} %shard_map.83), calls=%async_computation.2 | async-start | bytes 1048576 | tf_op jit(solution)/shard_map/all_to_all | solution.py:185
  240.3 8.0 %copy-start.4 = (f32[1024]{0:T(1024)S(1)}, f32[1024]{0:T(1024)}, u32[]{:S(2)}) copy-start(f32[1024]{0:T(1024)} %param.15) | copy-start | bytes 12292

commit v3 on v1

v3 whole, which is shorter than its diff:
```python
import functools

import jax
import jax.numpy as jnp
from jax import lax
from jax.experimental import pallas as pl
from jax.experimental.pallas import tpu as pltpu
from jax.sharding import PartitionSpec as P

LAYERS = 2
IN_SCALE = 2.0**19
OUT_SCALE = 2.0**17
X_SCALE = 2.0**6


def exchanged(value, axis):
    size = lax.axis_size(axis)
    return lax.all_to_all(
        jnp.broadcast_to(value[None], (size, *value.shape)), axis, 0, 0, tiled=True
    )


def joined(pieces):
    size, rows, width = pieces.shape
    return jnp.moveaxis(pieces, 0, 1).reshape(rows, size * width)


def neighbours(block, axis, width):
    count = lax.axis_size(axis)
    forward = [(i, i + 1) for i in range(count - 1)]
    backward = [(i + 1, i) for i in range(count - 1)]
    low = lax.ppermute(block[block.shape[0] - width :], axis, forward)
    high = lax.ppermute(block[:width], axis, backward)
    return low, high


def packed_kernel(paired, order_ref, value_ref, gate_ref, out_ref, sent_ref):
    rows, channels = value_ref.shape[1:]
    out_rows, features = out_ref.shape[1:]
    half = channels // 2
    upper = order_ref[0] != 0
    at = 0

    def projection(layer, lower):
        lanes = slice(0, half) if lower else slice(half, channels)
        pair = value_ref[layer, :, lanes], gate_ref[layer, :, lanes]
        return [p.astype(jnp.float32) * IN_SCALE for p in pair]

    for layer in range(LAYERS):
        blocks = [projection(layer, True), projection(layer, False)]
        if paired and layer == LAYERS - 1:
            blocks = [[jnp.where(upper, high, low) for low, high in zip(*blocks)]]
        for value, gate in blocks:
            sent_ref[at : at + rows, :half] = value.astype(jnp.bfloat16)
            sent_ref[at : at + rows, half:] = gate.astype(jnp.bfloat16)
            at += rows
        for i in range(0, features, channels):
            block = out_ref[layer, :, i : i + channels].astype(jnp.float32) * OUT_SCALE
            sent_ref[at : at + out_rows] = block.astype(jnp.bfloat16)
            at += out_rows


def packed(value, gate, out, order, paired):
    rows, channels = value.shape[1:]
    out_rows, features = out.shape[1:]
    slices, at = [], 0
    for layer in range(LAYERS):
        of_layer = []
        for _ in range(1 if paired and layer == LAYERS - 1 else 2):
            of_layer.append(slice(at, at + rows))
            at += rows
        of_layer.append(slice(at, at + out_rows * (features // channels)))
        at = of_layer[-1].stop
        slices.append(of_layer)
    vmem = pl.BlockSpec(memory_space=pltpu.VMEM)
    sent = pl.pallas_call(
        functools.partial(packed_kernel, paired),
        out_shape=jax.ShapeDtypeStruct((at, channels), jnp.bfloat16),
        in_specs=[pl.BlockSpec(memory_space=pltpu.SMEM), vmem, vmem, vmem],
        out_specs=vmem,
    )(order.reshape(1), value, gate, out)
    return sent, slices


def out_product(act, block, rows):
    parts, height, width = block.shape
    return jnp.concatenate(
        [
            jnp.dot(
                act,
                block[:, i : i + rows].reshape(parts * rows, width),
                preferred_element_type=jnp.float32,
            )
            for i in range(0, height, rows)
        ],
        axis=1,
    ) * (1 / OUT_SCALE)


def split_in_three(value):
    parts = []
    for _ in range(3):
        part = lax.reduce_precision(value, 8, 7)
        parts.append(part.astype(jnp.bfloat16))
        value = value - part
    return parts


def convolved_kernel(
    first, order_ref, x_ref, a_ref, b_ref, gain_ref, taps_ref, out_ref,
    scaled_ref, squares_ref, total_ref, glu_ref,
):
    step = pl.program_id(0)
    _, rows_in, width = x_ref.shape
    count, rows, channels = out_ref.shape
    half = channels // 2
    block = 32
    blocks = range(0, rows_in, block)

    @pl.when(step == 0)
    def _():
        squares_ref[...] = jnp.zeros_like(squares_ref)
        total_ref[...] = jnp.zeros_like(total_ref)

    for at in blocks:
        square = squares_ref[at : at + block]
        for b in range(0, width, 128):
            xf = x_ref[0, at : at + block, b : b + 128].astype(jnp.float32)
            square = square + xf * xf
            scaled = (xf * gain_ref[0, :, b : b + 128]).astype(jnp.bfloat16)
            scaled_ref[at : at + block, b : b + 128] = scaled
        squares_ref[at : at + block] = square
    for k, w_ref in enumerate((a_ref, b_ref)):
        total_ref[k] += jnp.dot(scaled_ref[...], w_ref[0], preferred_element_type=jnp.float32)

    @pl.when(step == pl.num_programs(0) - 1)
    def _():
        swapped = order_ref[0] != 0
        for at in blocks:
            mean = jnp.sum(squares_ref[at : at + block], axis=1, keepdims=True)
            mean = mean / (pl.num_programs(0) * width)
            scale = lax.rsqrt(mean + 1e-06) * (1 / IN_SCALE)
            glu = []
            for k in range(2):
                value = total_ref[k, at : at + block, :half] * scale
                gate = total_ref[k, at : at + block, half:] * scale
                gated = (value * jax.nn.sigmoid(gate)).astype(jnp.bfloat16)
                glu.append(gated.astype(jnp.float32))
            glu_ref[0, at : at + block, :half] = jnp.where(swapped, glu[1], glu[0])
            glu_ref[0, at : at + block, half:] = jnp.where(swapped, glu[0], glu[1])
        reach_rows = rows_in - 8
        for shift in range(1, 8):
            glu_ref[shift, :reach_rows, :] = glu_ref[0, shift : shift + reach_rows, :]

        def convolve(i, carry):
            base = pl.multiple_of(i * block, block)
            for lane in range(0, channels, 128):
                lanes = slice(lane, lane + 128)
                conv = jnp.zeros((block, 128), jnp.float32)
                for tap in range(taps_ref.shape[0]):
                    down, shift = divmod(first + tap, 8)
                    moved = glu_ref[shift, pl.ds(pl.multiple_of(base + 8 * down, 8), block), lanes]
                    conv = conv + taps_ref[tap : tap + 1, lanes] * moved
                conv = conv.astype(jnp.bfloat16)
                for c in range(count):
                    out_ref[c, pl.ds(base, block), lanes] = conv
            return carry

        lax.fori_loop(0, rows // block, convolve, 0)


def convolved(pieces, blocks, order, gain, taps, rows):
    count, rows_in, width = pieces.shape
    channels = taps.shape[1]
    first = (rows_in - rows) // 2 - taps.shape[0] // 2
    blocks = [b.reshape(count, width, channels) for b in blocks]
    along = lambda *shape: pl.BlockSpec((1, *shape), lambda j: (j, 0, 0))
    return pl.pallas_call(
        functools.partial(convolved_kernel, first),
        grid=(count,),
        out_shape=jax.ShapeDtypeStruct((count, rows, channels), jnp.bfloat16),
        in_specs=[
            pl.BlockSpec(memory_space=pltpu.SMEM),
            along(rows_in, width),
            along(width, channels),
            along(width, channels),
            along(1, width),
            pl.BlockSpec(taps.shape, lambda j: (0, 0)),
        ],
        out_specs=pl.BlockSpec((count, rows, channels), lambda j: (0, 0, 0)),
        scratch_shapes=[
            pltpu.VMEM((rows_in, width), jnp.bfloat16),
            pltpu.VMEM((rows_in, 128), jnp.float32),
            pltpu.VMEM((2, rows_in, channels), jnp.float32),
            pltpu.VMEM((8, rows_in, channels), jnp.float32),
        ],
        cost_estimate=pl.CostEstimate(
            flops=4 * rows_in * count * width * channels,
            bytes_accessed=4 * count * width * channels + 2 * count * rows_in * width,
            transcendentals=rows_in * channels,
        ),
    )(order.reshape(1), pieces, *blocks, gain.reshape(count, 1, width), taps)


def activated(conv, gain):
    conv = conv.astype(jnp.float32)
    center = jnp.mean(conv, axis=1, keepdims=True)
    shifted = conv - center
    spread = jnp.mean(shifted * shifted, axis=1, keepdims=True)
    return jax.nn.silu(shifted * lax.rsqrt(spread + 1e-05) * gain[None, :]).astype(jnp.bfloat16)


def on_device(
    tokens, norm_gain, value_weight, gate_weight, conv_taps, channel_gain, out_weight, final_gain
):
    rows = tokens.shape[0]
    margin = 16
    low, high = neighbours(tokens, "sp", 2 * margin)
    coded = jnp.stack(split_in_three(channel_gain)).reshape(-1)
    width = tokens.shape[1]
    coded = jnp.pad(coded, (0, 2 * width - coded.shape[0])).reshape(2, width)
    x_local = jnp.concatenate([low, tokens, high], axis=0)
    everyone = exchanged(jnp.concatenate([coded[:1], x_local[1:-1], coded[1:]], axis=0), "tp")
    x_local = x_local[margin:-margin]
    gains = jnp.concatenate([everyone[:, 0], everyone[:, -1]], axis=1)[:, : 3 * channel_gain.size]
    gains = gains.reshape(-1, 3, *channel_gain.shape).astype(jnp.float32)
    gains = gains[:, 0] + (gains[:, 1] + gains[:, 2])
    gains = jnp.moveaxis(gains, 0, 1).reshape(LAYERS, -1)
    groups = lax.axis_size("grp")
    paired = groups % 2 == 0
    order = lax.axis_index("grp") % 2 if paired else jnp.int32(0)
    swap = [(i, i ^ 1) for i in range(groups)]
    out_rows = out_weight.shape[1]
    sent, slices = packed(value_weight, gate_weight, out_weight, order, paired)
    weights = lax.all_gather(sent.astype(jnp.float16), "sp")

    def taken(at):
        return weights[:, at].astype(jnp.bfloat16)

    late_blocks = [taken(at) for at in slices[1][:-1]]
    if paired:
        late_blocks.append(lax.ppermute(late_blocks[0], "grp", swap))
    middle = rows + 2 * margin
    conv = convolved(
        everyone, [taken(at) for at in slices[0][:-1]], jnp.int32(0), norm_gain[0], conv_taps[0], middle
    )
    conv, weights = lax.optimization_barrier((conv, weights))
    conv_all = joined(lax.all_to_all(conv, "tp", 0, 0, tiled=True))
    act = activated(conv_all, gains[0])
    branch = out_product(act, taken(slices[0][-1]), out_rows)
    position = lax.axis_index("sp") * rows - margin + lax.iota(jnp.int32, middle)
    inside = (position >= 0) & (position < rows * lax.axis_size("sp"))
    x_next = x_local.astype(jnp.float32) + branch
    x_next = jnp.where(inside[:, None], x_next, 0.0).astype(jnp.bfloat16)

    shared = (x_next.astype(jnp.float32) * X_SCALE).astype(jnp.float16)
    x_all = lax.all_gather(shared, "tp").astype(jnp.float32) * (1 / X_SCALE)
    conv = convolved(
        x_all.astype(jnp.bfloat16), late_blocks, order, norm_gain[1], conv_taps[1], rows
    )
    conv, weights = lax.optimization_barrier((conv, weights))
    conv_all = joined(lax.all_to_all(conv, "tp", 0, 0, tiled=True))
    act = activated(conv_all, gains[1])
    branch = out_product(act, taken(slices[1][-1]), out_rows)
    x_last = (x_next[margin : margin + rows].astype(jnp.float32) + branch).astype(jnp.bfloat16)

    xf = x_last.astype(jnp.float32)
    squares = jnp.sum(exchanged(jnp.sum(xf * xf, axis=1), "tp"), axis=0)
    width = xf.shape[1] * lax.axis_size("tp")
    scale = lax.rsqrt(squares / width + 1e-06)[:, None]
    return (xf * scale * final_gain[None, :]).astype(jnp.bfloat16)


def solution(mesh):
    placed = (
        P(("grp", "sp"), "tp"),
        P(),
        P(None, "sp", "tp"),
        P(None, "sp", "tp"),
        P(None, None, "tp"),
        P(None, "tp"),
        P(None, "sp", "tp"),
        P("tp"),
    )
    return jax.shard_map(
        on_device, mesh=mesh, in_specs=placed, out_specs=P(("grp", "sp"), "tp"), check_vma=False
    )
```

time: 257 us -> 245 us (0.953)
  Pallas kernels: 0 us -> 15.3 us
  other arithmetic: 29.6 us -> 16.4 us
  blocking collectives: 175 us -> 166 us
  local copies, waits for them, and re-layouts: 16 us -> 9.96 us
  matrix products: 7.73 us -> 3.66 us
  waiting for transfers between devices: 9.14 us -> 13.2 us
    pallas_call x0 -> x3, Pallas kernels: none -> 15.3 us  [the longest x2 13.7 us: convolved(): pl.pallas_call(functools.partial(convolved_kernel, first), grid=(count,),...]
    all_to_all x0 -> x2, waiting for transfers between devices: none -> 12.3 us  [on_device(): conv_all = joined(lax.all_to_all(conv, 'tp', 0, 0, tiled=True))]
    all_gather x2, blocking collectives: 167 us -> 158 us  [the longest x1 135 us: on_device(): weights = lax.all_gather(sent.astype(jnp.float16), 'sp')]
    all_to_all x3 -> x1, starting transfers between devices: 13.8 us -> 4.58 us  [exchanged(): lax.all_to_all(jnp.broadcast_to(value[None], (size, *value.shape)), axis,...]
    all_to_all x3 -> x1, waiting for transfers between devices: 9.13 us -> 0.01 us  [exchanged(): lax.all_to_all(jnp.broadcast_to(value[None], (size, *value.shape)), axis,...]
    convert_element_type x11 -> x6, other arithmetic: 21.2 us -> 12.5 us  [the longest x3 8.95 us: taken(): return weights[:, at].astype(jnp.bfloat16)]
    all_to_all x0 -> x2, starting transfers between devices: none -> 8.55 us  [on_device(): conv_all = joined(lax.all_to_all(conv, 'tp', 0, 0, tiled=True))]
    dot_general x6 -> x8, matrix products: 7.73 us -> 3.66 us  [out_product(): jnp.dot(act, block[:, i:i + rows].reshape(parts * rows, width), preferred...]
  transfers between devices with their start and end apart: 5 -> 6, of which waited for: 2 -> 3; matrix products, arithmetic and copies ran while one was open for 10% -> 8% of each run, Pallas kernels for 0% -> 4%
where the time goes in v3:
time: 245 us; the launch traced here: 243 us
  blocking collectives  166 us (68%)
  starting transfers between devices  18.2 us (7%)
  other arithmetic  16.4 us (7%)
  Pallas kernels  15.3 us (6%)
  waiting for transfers between devices  13.2 us (5%)
  local copies, waits for them, and re-layouts  9.96 us (4%)
  matrix products  3.66 us (1%)
    all_gather x1, blocking collectives, on_device(): weights = lax.all_gather(sent.astype(jnp.float16), 'sp')  135 us
    all_gather x1, blocking collectives, on_device(): x_all = lax.all_gather(shared, 'tp').astype(jnp.float32) * (1 / X_SCALE)  22.7 us
    pallas_call x2, Pallas kernels, convolved(): pl.pallas_call(functools.partial(convolved_kernel, first), grid=(count,),...  13.7 us
    all_to_all x2, waiting for transfers between devices, on_device(): conv_all = joined(lax.all_to_all(conv, 'tp', 0, 0, tiled=True))  12.3 us
    convert_element_type x3, other arithmetic, taken(): return weights[:, at].astype(jnp.bfloat16)  8.95 us
    all_to_all x2, starting transfers between devices, on_device(): conv_all = joined(lax.all_to_all(conv, 'tp', 0, 0, tiled=True))  8.55 us
    all_to_all x1, blocking collectives, exchanged(): lax.all_to_all(jnp.broadcast_to(value[None], (size, *value.shape)), axis,...  7.67 us
  transfers between devices with their start and end apart: 6, of which 3 were waited for; matrix products, arithmetic and copies ran while one was open for 8% of the time, Pallas kernels for 4%

profile of v3, /device:TPU:40, one launch (start us, length us, event | category | flops | bytes accessed | tf_op | source)
XLA Modules:
  0.0 242.8 jit_solution(15029670144251658836)
XLA Ops:
  0.0 0.9 fusion.46
  0.9 1.8 collective-permute-start
  2.8 1.3 collective-permute-start.1
  4.1 0.7 fusion.38
  4.9 1.6 shard_map.82
  6.5 0.9 convert_element_type.107
  7.5 0.9 collective-permute-done.1
  8.6 0.2 pad_maximum_fusion
  8.8 1.9 broadcast_in_dim.17
  10.7 4.6 %all-to-all-start = ((bf16[4,320,1024]{2,1,0:T(8,128)(2,1)}), bf16[4,320,1024]{2,1,0:T(8,128)(2,1)S(1)}, u32[]{:S(2)}, u32[]{:S(2)}) async-start(bf16[4,320,1024]{2,1,0:T(8,128)(2,1)} %broadcast_in_dim.17), calls=%async_computation | async-start | bytes 5242880 | tf_op jit(solution)/shard_map/all_to_all | solution.py:18
  15.3 135.3 %all-gather.4 = f16[20480,256]{1,0:T(8,128)(2,1)S(1)} all-gather(f16[320,256]{1,0:T(8,128)(2,1)S(1)} %convert_element_type.107), channel_id=2, replica_groups=mesh['grp'=2,'sp'=64,'tp'=4] {'sp'}, dimensions={0}, use_global_device_ids=true | all-gather | bytes 10649600 | tf_op jit(solution)/shard_map/all_gather | solution.py:235
  150.6 4.7 %slice_convert_fusion = (bf16[64,64,256]{2,1,0:T(8,128)(2,1)}, bf16[64,64,256]{2,1,0:T(8,128)(2,1)}, bf16[64,64,256]{2,1,0:T(8,128)(2,1)}) fusion(f16[64,320,256]{2,1,0:T(8,128)(2,1)S(1)} %bitcast.101), kind=kLoop, calls=%fused_computation.1 | loop fusion | flops 3145728 | bytes 12582912 | tf_op jit(solution)/shard_map/convert_element_type | solution.py:238
  155.3 1.1 copy-done
  156.4 1.9 collective-permute-start.2
  158.4 0.6 copy.81
  159.0 0.6 copy.80
  159.6 0.6 fusion.48
  160.3 1.5 copy-done.1
  161.8 7.0 %shard_map.83 = bf16[4,288,256]{2,1,0:T(8,128)(2,1)} custom-call(s32[1]{0:T(128)} %constant.52.clone.1.order_ref, bf16[4,320,1024]{2,1,0:T(8,128)(2,1)} %copy-done.1, bf16[4,1024,256]{2,1,0:T(8,128)(2,1)} %bitcast.114, bf16[4,1024,256]{2,1,0:T(8,128)(2,1)} %bitcast.113, f32[4,1,1024]{2,1,0:T(1,128)} %bitcast.126, f32[31,256]{1,0:T(8,128)} %bitcast.124), custom_call_target="tpu_custom_call" | custom-call | flops 1342177280 | bytes 6815744 | tf_op jit(solution)/shard_map/pallas_call | solution.py:178
  168.8 4.8 %all-to-all-start.1 = ((bf16[4,288,256]{2,1,0:T(8,128)(2,1)}), bf16[4,288,256]{2,1,0:T(8,128)(2,1)S(1)}, u32[]{:S(2)}, u32[]{:S(2)}) async-start(bf16[4,288,256]{2,1,0:T(8,128)(2,1)} %shard_map.83), calls=%async_computation.1 | async-start | bytes 1179648 | tf_op jit(solution)/shard_map/all_to_all | solution.py:248
  173.6 0.9 fusion.43
  174.6 2.1 slice_convert_fusion.4
  176.7 0.2 fusion.45
  176.9 7.4 %all-to-all-done.1 = bf16[4,288,256]{2,1,0:T(8,128)(2,1)S(1)} async-done(((bf16[4,288,256]{2,1,0:T(8,128)(2,1)}), bf16[4,288,256]{2,1,0:T(8,128)(2,1)S(1)}, u32[]{:S(2)}, u32[]{:S(2)}) %all-to-all-start.1) | async-done | bytes 589856 | tf_op jit(solution)/shard_map/all_to_all | solution.py:248
  184.5 0.3 fusion.4
  184.8 0.5 fusion.30
  185.4 0.3 fusion.52
  185.7 0.3 fusion.51
  186.0 0.3 fusion.50
  186.4 0.3 fusion.49
  186.7 0.3 multiply_convert_fusion.1
  187.0 22.7 %all-gather.5 = f16[1152,1024]{1,0:T(8,128)(2,1)S(1)} all-gather(f16[288,1024]{1,0:T(8,128)(2,1)S(1)} %get-tuple-element.15), channel_id=3, replica_groups=mesh['grp'=2,'sp'=64,'tp'=4] {'tp'}, dimensions={0}, use_global_device_ids=true | all-gather | bytes 2949120 | tf_op jit(solution)/shard_map/all_gather | solution.py:257
  209.7 2.1 multiply_convert_fusion
  211.8 6.7 %shard_map.84 = bf16[4,256,256]{2,1,0:T(8,128)(2,1)} custom-call(s32[1]{0:T(128)} %bitcast.3.order_ref, bf16[4,288,1024]{2,1,0:T(8,128)(2,1)} %bitcast.112, bf16[4,1024,256]{2,1,0:T(8,128)(2,1)} %bitcast.21.a_ref, bf16[4,1024,256]{2,1,0:T(8,128)(2,1)} %bitcast.22.b_ref, f32[4,1,1024]{2,1,0:T(1,128)} %bitcast.125, f32[31,256]{1,0:T(8,128)} %bitcast.123), custom_call_target="tpu_custom_call" | custom-call | flops 1207959552 | bytes 6553600 | tf_op jit(solution)/shard_map/pallas_call | solution.py:178
  218.5 3.7 %all-to-all-start.2 = ((bf16[4,256,256]{2,1,0:T(8,128)(2,1)}), bf16[4,256,256]{2,1,0:T(8,128)(2,1)S(1)}, u32[]{:S(2)}, u32[]{:S(2)}) async-start(bf16[4,256,256]{2,1,0:T(8,128)(2,1)} %shard_map.84), calls=%async_computation.2 | async-start | bytes 1048576 | tf_op jit(solution)/shard_map/all_to_all | solution.py:262
  222.2 2.1 slice_convert_fusion.3
  224.4 1.0 fusion.44
  225.4 4.9 %all-to-all-done.2 = bf16[4,256,256]{2,1,0:T(8,128)(2,1)S(1)} async-done(((bf16[4,256,256]{2,1,0:T(8,128)(2,1)}), bf16[4,256,256]{2,1,0:T(8,128)(2,1)S(1)}, u32[]{:S(2)}, u32[]{:S(2)}) %all-to-all-start.2) | async-done | bytes 524320 | tf_op jit(solution)/shard_map/all_to_all | solution.py:262
  230.4 0.3 fusion.16
  230.7 0.5 fusion.24
  231.2 0.2 copy.58
  231.4 1.4 fusion.56
  232.8 0.3 fusion.55
  233.1 0.3 fusion.54
  233.5 0.3 fusion.53
  233.8 0.3 fusion.25
  234.1 7.7 %all_to_all.21 = f32[4,1,256]{2,1,0:T(1,128)S(1)} all-to-all(f32[4,1,256]{2,1,0:T(1,128)S(1)} %broadcast_in_dim.19), channel_id=1, replica_groups=mesh['grp'=2,'sp'=64,'tp'=4] {'tp'}, dimensions={0} | all-to-all | bytes 8192 | tf_op jit(solution)/shard_map/all_to_all | solution.py:18
  241.8 1.0 fusion.27
  (40 shorter events, 0.8 us)
Async XLA Ops:
  0.0 7.5 %copy-start.2 = (bf16[256,1024]{1,0:T(8,128)(2,1)S(1)}, bf16[256,1024]{1,0:T(8,128)(2,1)}, u32[]{:S(2)}) copy-start(bf16[256,1024]{1,0:T(8,128)(2,1)} %param.8) | copy-start | bytes 1572868
  0.9 6.5 %collective-permute-start = (bf16[32,1024]{1,0:T(8,128)(2,1)S(1)}, bf16[32,1024]{1,0:T(8,128)(2,1)S(1)}, u32[]{:S(2)}, u32[]{:S(2)}) collective-permute-start(bf16[32,1024]{1,0:T(8,128)(2,1)S(1)} %get-tuple-element.31), channel_id=1, source_target_pairs={{0,4},{4,8},{8,12},{12,16},{16,20},{20,24},{24,28},{28,32},{32,36}... | collective-permute-start | bytes 196616 | tf_op jit(solution)/shard_map/ppermute | solution.py:32
  2.8 5.7 %collective-permute-start.1 = (bf16[32,1024]{1,0:T(8,128)(2,1)S(1)}, bf16[32,1024]{1,0:T(8,128)(2,1)S(1)}, u32[]{:S(2)}, u32[]{:S(2)}) collective-permute-start(bf16[32,1024]{1,0:T(8,128)(2,1)S(1)} %get-tuple-element.30), channel_id=1, source_target_pairs={{4,0},{8,4},{12,8},{16,12},{20,16},{24,20},{28,24},{32,28},{36,32}... | collective-permute-start | bytes 196616 | tf_op jit(solution)/shard_map/ppermute | solution.py:33
  10.7 149.6 %all-to-all-start = ((bf16[4,320,1024]{2,1,0:T(8,128)(2,1)}), bf16[4,320,1024]{2,1,0:T(8,128)(2,1)S(1)}, u32[]{:S(2)}, u32[]{:S(2)}) async-start(bf16[4,320,1024]{2,1,0:T(8,128)(2,1)} %broadcast_in_dim.17), calls=%async_computation | async-start | bytes 5242880 | tf_op jit(solution)/shard_map/all_to_all | solution.py:18
  150.6 5.8 %copy-start = (f16[20480,256]{1,0:T(8,128)(2,1)}, f16[20480,256]{1,0:T(8,128)(2,1)S(1)}, u32[]{:S(2)}) copy-start(f16[20480,256]{1,0:T(8,128)(2,1)S(1)} %all-gather.4) | copy-start | bytes 31457284
  150.6 7.7 %copy-start.3 = (f32[2,31,256]{2,0,1:T(2,128)S(1)}, f32[2,31,256]{2,0,1:T(2,128)}, u32[]{:S(2)}) copy-start(f32[2,31,256]{2,0,1:T(2,128)} %param.12) | copy-start | bytes 190468
  150.6 9.0 %copy-start.4 = (f32[2,4096]{1,0:T(2,128)S(1)}, f32[2,4096]{1,0:T(2,128)}, u32[]{:S(2)}) copy-start(f32[2,4096]{1,0:T(2,128)} %param.9) | copy-start | bytes 98308
  156.4 55.5 %collective-permute-start.2 = (bf16[64,64,256]{2,1,0:T(8,128)(2,1)}, bf16[64,64,256]{2,1,0:T(8,128)(2,1)}, u32[]{:S(2)}, u32[]{:S(2)}) collective-permute-start(bf16[64,64,256]{2,1,0:T(8,128)(2,1)} %get-tuple-element.17), channel_id=1, source_target_pairs={{0,256},{256,0},{1,257},{257,1},{2,258},{258,2},{3,259},{259,3},{4... | collective-permute-start | bytes 6291464 | tf_op jit(solution)/shard_map/ppermute | solution.py:242
  160.2 1.5 copy-start.1
  168.8 15.5 %all-to-all-start.1 = ((bf16[4,288,256]{2,1,0:T(8,128)(2,1)}), bf16[4,288,256]{2,1,0:T(8,128)(2,1)S(1)}, u32[]{:S(2)}, u32[]{:S(2)}) async-start(bf16[4,288,256]{2,1,0:T(8,128)(2,1)} %shard_map.83), calls=%async_computation.1 | async-start | bytes 1179648 | tf_op jit(solution)/shard_map/all_to_all | solution.py:248
  218.5 11.8 %all-to-all-start.2 = ((bf16[4,256,256]{2,1,0:T(8,128)(2,1)}), bf16[4,256,256]{2,1,0:T(8,128)(2,1)S(1)}, u32[]{:S(2)}, u32[]{:S(2)}) async-start(bf16[4,256,256]{2,1,0:T(8,128)(2,1)} %shard_map.84), calls=%async_computation.2 | async-start | bytes 1048576 | tf_op jit(solution)/shard_map/all_to_all | solution.py:262
  233.8 8.0 %copy-start.5 = (f32[1024]{0:T(1024)S(1)}, f32[1024]{0:T(1024)}, u32[]{:S(2)}) copy-start(f32[1024]{0:T(1024)} %param.15) | copy-start | bytes 12292

commit v4 on v3

--- a/solution.py
+++ b/solution.py
@@ -6,6 +6,7 @@
 from jax.experimental import pallas as pl
 from jax.experimental.pallas import tpu as pltpu
 from jax.sharding import PartitionSpec as P
+
 
 LAYERS = 2
 IN_SCALE = 2.0**19
@@ -34,7 +35,7 @@
     return low, high
 
 
-def packed_kernel(paired, order_ref, value_ref, gate_ref, out_ref, sent_ref):
+def packed_kernel(paired, order_ref, value_ref, gate_ref, out_ref, chan_ref, sent_ref, coded_ref):
     rows, channels = value_ref.shape[1:]
     out_rows, features = out_ref.shape[1:]
     half = channels // 2
@@ -54,13 +55,25 @@
             sent_ref[at : at + rows, :half] = value.astype(jnp.bfloat16)
             sent_ref[at : at + rows, half:] = gate.astype(jnp.bfloat16)
             at += rows
-        for i in range(0, features, channels):
-            block = out_ref[layer, :, i : i + channels].astype(jnp.float32) * OUT_SCALE
+        starts = range(0, features, channels)
+        blocks = [out_ref[layer, :, i : i + channels].astype(jnp.float32) * OUT_SCALE for i in starts]
+        if paired and layer == LAYERS - 1:
+            middle = len(blocks) // 2
+            blocks = [jnp.where(upper, h, l) for l, h in zip(blocks[:middle], blocks[middle:])]
+        for block in blocks:
             sent_ref[at : at + out_rows] = block.astype(jnp.bfloat16)
             at += out_rows
-
-
-def packed(value, gate, out, order, paired):
+    coded_ref[...] = jnp.zeros_like(coded_ref)
+    for layer in range(LAYERS):
+        rest = chan_ref[layer : layer + 1, :]
+        for part in range(3):
+            row, lane = divmod((layer * 3 + part) * channels, coded_ref.shape[1])
+            coded = rest.astype(jnp.bfloat16)
+            coded_ref[row : row + 1, lane : lane + channels] = coded
+            rest = rest - coded.astype(jnp.float32)
+
+
+def packed(value, gate, out, chan_gain, order, paired):
     rows, channels = value.shape[1:]
     out_rows, features = out.shape[1:]
     slices, at = [], 0
@@ -69,17 +82,21 @@
         for _ in range(1 if paired and layer == LAYERS - 1 else 2):
             of_layer.append(slice(at, at + rows))
             at += rows
-        of_layer.append(slice(at, at + out_rows * (features // channels)))
+        share = 2 if paired and layer == LAYERS - 1 else 1
+        of_layer.append(slice(at, at + out_rows * (features // channels) // share))
         at = of_layer[-1].stop
         slices.append(of_layer)
     vmem = pl.BlockSpec(memory_space=pltpu.VMEM)
-    sent = pl.pallas_call(
+    sent, coded = pl.pallas_call(
         functools.partial(packed_kernel, paired),
-        out_shape=jax.ShapeDtypeStruct((at, channels), jnp.bfloat16),
-        in_specs=[pl.BlockSpec(memory_space=pltpu.SMEM), vmem, vmem, vmem],
-        out_specs=vmem,
-    )(order.reshape(1), value, gate, out)
-    return sent, slices
+        out_shape=(
+            jax.ShapeDtypeStruct((at, channels), jnp.bfloat16),
+            jax.ShapeDtypeStruct((2, features), jnp.bfloat16),
+        ),
+        in_specs=[pl.BlockSpec(memory_space=pltpu.SMEM), vmem, vmem, vmem, vmem],
+        out_specs=(vmem, vmem),
+    )(order.reshape(1), value, gate, out, chan_gain)
+    return sent, coded, slices
 
 
 def out_product(act, block, rows):
@@ -97,17 +114,8 @@
     ) * (1 / OUT_SCALE)
 
 
-def split_in_three(value):
-    parts = []
-    for _ in range(3):
-        part = lax.reduce_precision(value, 8, 7)
-        parts.append(part.astype(jnp.bfloat16))
-        value = value - part
-    return parts
-
-
 def convolved_kernel(
-    first, order_ref, x_ref, a_ref, b_ref, gain_ref, taps_ref, out_ref,
+    first, layer, order_ref, x_ref, a_ref, b_ref, gain_ref, taps_ref, out_ref,
     scaled_ref, squares_ref, total_ref, glu_ref,
 ):
     step = pl.program_id(0)
@@ -127,7 +135,7 @@
         for b in range(0, width, 128):
             xf = x_ref[0, at : at + block, b : b + 128].astype(jnp.float32)
             square = square + xf * xf
-            scaled = (xf * gain_ref[0, :, b : b + 128]).astype(jnp.bfloat16)
+            scaled = (xf * gain_ref[layer : layer + 1, b : b + 128]).astype(jnp.bfloat16)
             scaled_ref[at : at + block, b : b + 128] = scaled
         squares_ref[at : at + block] = square
     for k, w_ref in enumerate((a_ref, b_ref)):
@@ -160,7 +168,7 @@
                 for tap in range(taps_ref.shape[0]):
                     down, shift = divmod(first + tap, 8)
                     moved = glu_ref[shift, pl.ds(pl.multiple_of(base + 8 * down, 8), block), lanes]
-                    conv = conv + taps_ref[tap : tap + 1, lanes] * moved
+                    conv = conv + taps_ref[tap, layer : layer + 1, lanes] * moved
                 conv = conv.astype(jnp.bfloat16)
                 for c in range(count):
                     out_ref[c, pl.ds(base, block), lanes] = conv
@@ -169,14 +177,15 @@
         lax.fori_loop(0, rows // block, convolve, 0)
 
 
-def convolved(pieces, blocks, order, gain, taps, rows):
+def convolved(pieces, blocks, order, gains, taps, layer, rows):
     count, rows_in, width = pieces.shape
-    channels = taps.shape[1]
+    taps = jnp.moveaxis(taps, 0, 1)
+    channels = taps.shape[2]
     first = (rows_in - rows) // 2 - taps.shape[0] // 2
     blocks = [b.reshape(count, width, channels) for b in blocks]
     along = lambda *shape: pl.BlockSpec((1, *shape), lambda j: (j, 0, 0))
     return pl.pallas_call(
-        functools.partial(convolved_kernel, first),
+        functools.partial(convolved_kernel, first, layer),
         grid=(count,),
         out_shape=jax.ShapeDtypeStruct((count, rows, channels), jnp.bfloat16),
         in_specs=[
@@ -184,8 +193,8 @@
             along(rows_in, width),
             along(width, channels),
             along(width, channels),
-            along(1, width),
-            pl.BlockSpec(taps.shape, lambda j: (0, 0)),
+            pl.BlockSpec((gains.shape[0], width), lambda j: (0, j)),
+            pl.BlockSpec(taps.shape, lambda j: (0, 0, 0)),
         ],
         out_specs=pl.BlockSpec((count, rows, channels), lambda j: (0, 0, 0)),
         scratch_shapes=[
@@ -199,7 +208,7 @@
             bytes_accessed=4 * count * width * channels + 2 * count * rows_in * width,
             transcendentals=rows_in * channels,
         ),
-    )(order.reshape(1), pieces, *blocks, gain.reshape(count, 1, width), taps)
+    )(order.reshape(1), pieces, *blocks, gains, taps)
 
 
 def activated(conv, gain):
@@ -215,24 +224,20 @@
 ):
     rows = tokens.shape[0]
     margin = 16
-    low, high = neighbours(tokens, "sp", 2 * margin)
-    coded = jnp.stack(split_in_three(channel_gain)).reshape(-1)
-    width = tokens.shape[1]
-    coded = jnp.pad(coded, (0, 2 * width - coded.shape[0])).reshape(2, width)
-    x_local = jnp.concatenate([low, tokens, high], axis=0)
-    everyone = exchanged(jnp.concatenate([coded[:1], x_local[1:-1], coded[1:]], axis=0), "tp")
-    x_local = x_local[margin:-margin]
-    gains = jnp.concatenate([everyone[:, 0], everyone[:, -1]], axis=1)[:, : 3 * channel_gain.size]
-    gains = gains.reshape(-1, 3, *channel_gain.shape).astype(jnp.float32)
-    gains = gains[:, 0] + (gains[:, 1] + gains[:, 2])
-    gains = jnp.moveaxis(gains, 0, 1).reshape(LAYERS, -1)
     groups = lax.axis_size("grp")
     paired = groups % 2 == 0
     order = lax.axis_index("grp") % 2 if paired else jnp.int32(0)
     swap = [(i, i ^ 1) for i in range(groups)]
     out_rows = out_weight.shape[1]
-    sent, slices = packed(value_weight, gate_weight, out_weight, order, paired)
+    sent, coded, slices = packed(
+        value_weight, gate_weight, out_weight, channel_gain, order, paired
+    )
+    low, high = neighbours(tokens, "sp", 2 * margin)
+    x_local = jnp.concatenate([low, tokens, high], axis=0)
+    everyone = exchanged(jnp.concatenate([coded[:1], x_local[1:-1], coded[1:]], axis=0), "tp")
+    x_local = x_local[margin:-margin]
     weights = lax.all_gather(sent.astype(jnp.float16), "sp")
+    weights, everyone = lax.optimization_barrier((weights, everyone))
 
     def taken(at):
         return weights[:, at].astype(jnp.bfloat16)
@@ -242,10 +247,23 @@
         late_blocks.append(lax.ppermute(late_blocks[0], "grp", swap))
     middle = rows + 2 * margin
     conv = convolved(
-        everyone, [taken(at) for at in slices[0][:-1]], jnp.int32(0), norm_gain[0], conv_taps[0], middle
+        everyone,
+        [taken(at) for at in slices[0][:-1]],
+        jnp.int32(0),
+        norm_gain,
+        conv_taps,
+        0,
+        middle,
     )
     conv, weights = lax.optimization_barrier((conv, weights))
+    late_outs = [taken(slices[1][-1])]
+    if paired:
+        late_outs.append(lax.ppermute(late_outs[0], "grp", swap))
     conv_all = joined(lax.all_to_all(conv, "tp", 0, 0, tiled=True))
+    gains = jnp.concatenate([everyone[:, 0], everyone[:, -1]], axis=1)[:, : 3 * channel_gain.size]
+    gains = gains.reshape(-1, LAYERS, 3, channel_gain.shape[1]).astype(jnp.float32)
+    gains = gains[:, :, 0] + (gains[:, :, 1] + gains[:, :, 2])
+    gains = jnp.moveaxis(gains, 0, 1).reshape(LAYERS, -1)
     act = activated(conv_all, gains[0])
     branch = out_product(act, taken(slices[0][-1]), out_rows)
     position = lax.axis_index("sp") * rows - margin + lax.iota(jnp.int32, middle)
@@ -256,12 +274,15 @@
     shared = (x_next.astype(jnp.float32) * X_SCALE).astype(jnp.float16)
     x_all = lax.all_gather(shared, "tp").astype(jnp.float32) * (1 / X_SCALE)
     conv = convolved(
-        x_all.astype(jnp.bfloat16), late_blocks, order, norm_gain[1], conv_taps[1], rows
-    )
-    conv, weights = lax.optimization_barrier((conv, weights))
+        x_all.astype(jnp.bfloat16), late_blocks, order, norm_gain, conv_taps, 1, rows
+    )
     conv_all = joined(lax.all_to_all(conv, "tp", 0, 0, tiled=True))
     act = activated(conv_all, gains[1])
-    branch = out_product(act, taken(slices[1][-1]), out_rows)
+    branches = [out_product(act, o, out_rows) for o in late_outs]
+    if paired:
+        own, other = branches
+        branches = [jnp.where(order == 0, own, other), jnp.where(order == 0, other, own)]
+    branch = jnp.concatenate(branches, axis=1)
     x_last = (x_next[margin : margin + rows].astype(jnp.float32) + branch).astype(jnp.bfloat16)
 
     xf = x_last.astype(jnp.float32)
@@ -282,6 +303,7 @@
         P(None, "sp", "tp"),
         P("tp"),
     )
+
     return jax.shard_map(
         on_device, mesh=mesh, in_specs=placed, out_specs=P(("grp", "sp"), "tp"), check_vma=False
     )

time: 245 us -> 262 us (1.069)
  waiting for transfers between devices: 13.2 us -> 23.1 us
  other arithmetic: 16.4 us -> 22 us
  starting transfers between devices: 18.2 us -> 23.4 us
  blocking collectives: 166 us -> 163 us
    ppermute x1, waiting for transfers between devices: 0.01 us -> 10.5 us  [on_device(): late_blocks.append(lax.ppermute(late_blocks[0], 'grp', swap))]
    all_to_all x2, waiting for transfers between devices: 12.3 us -> 1.81 us  [on_device(): conv_all = joined(lax.all_to_all(conv, 'tp', 0, 0, tiled=True))]
    ppermute x0 -> x1, waiting for transfers between devices: none -> 9.8 us  [on_device(): late_outs.append(lax.ppermute(late_outs[0], 'grp', swap))]
    convert_element_type x3, other arithmetic: 8.95 us -> 14.4 us  [taken(): return weights[:, at].astype(jnp.bfloat16)]
    all_gather x1, blocking collectives: 135 us -> 131 us  [on_device(): weights = lax.all_gather(sent.astype(jnp.float16), 'sp')]
    ppermute x0 -> x1, starting transfers between devices: none -> 3.95 us  [on_device(): late_outs.append(lax.ppermute(late_outs[0], 'grp', swap))]
    slice x2 -> x3, local copies, waits for them, and re-layouts: 1.18 us -> 4.25 us  [out_product(): block[:, i:i + rows].reshape(parts * rows, width)]
  transfers between devices with their start and end apart: 6 -> 7, of which waited for: 3 -> 4; matrix products, arithmetic and copies ran while one was open for 8% -> 4% of each run, Pallas kernels for 4% -> 3%
where the time goes in v4:
time: 262 us; the launch traced here: 261 us
  blocking collectives  163 us (62%)
  starting transfers between devices  23.4 us (9%)
  waiting for transfers between devices  23.1 us (9%)
  other arithmetic  22 us (8%)
  Pallas kernels  15.4 us (6%)
  local copies, waits for them, and re-layouts  10.3 us (4%)
  matrix products  2.62 us (1%)
    all_gather x1, blocking collectives, on_device(): weights = lax.all_gather(sent.astype(jnp.float16), 'sp')  131 us
    all_gather x1, blocking collectives, on_device(): x_all = lax.all_gather(shared, 'tp').astype(jnp.float32) * (1 / X_SCALE)  22.7 us
    convert_element_type x3, other arithmetic, taken(): return weights[:, at].astype(jnp.bfloat16)  14.4 us
    pallas_call x2, Pallas kernels, convolved(): pl.pallas_call(functools.partial(convolved_kernel, first, layer), grid=(c...  13.8 us
    ppermute x1, waiting for transfers between devices, on_device(): late_blocks.append(lax.ppermute(late_blocks[0], 'grp', swap))  10.5 us
    ppermute x1, waiting for transfers between devices, on_device(): late_outs.append(lax.ppermute(late_outs[0], 'grp', swap))  9.8 us
    all_to_all x2, starting transfers between devices, on_device(): conv_all = joined(lax.all_to_all(conv, 'tp', 0, 0, tiled=True))  9.76 us
    all_to_all x1, blocking collectives, exchanged(): lax.all_to_all(jnp.broadcast_to(value[None], (size, *value.shape)), axis,...  9.63 us
  transfers between devices with their start and end apart: 7, of which 4 were waited for; matrix products, arithmetic and copies ran while one was open for 4% of the time, Pallas kernels for 3%

profile of v4, /device:TPU:40, one launch (start us, length us, event | category | flops | bytes accessed | tf_op | source)
XLA Modules:
  0.0 260.7 jit_solution(9660848382827146571)
XLA Ops:
  0.0 0.9 fusion.43
  0.9 1.8 collective-permute-start
  2.8 1.3 collective-permute-start.1
  4.1 1.6 shard_map.82
  5.7 0.8 fusion.44
  6.5 0.9 convert_element_type.93
  7.5 0.9 collective-permute-done.1
  8.8 1.8 broadcast_in_dim.17
  10.6 4.6 %all-to-all-start = ((bf16[4,320,1024]{2,1,0:T(8,128)(2,1)}), bf16[4,320,1024]{2,1,0:T(8,128)(2,1)S(1)}, u32[]{:S(2)}, u32[]{:S(2)}) async-start(bf16[4,320,1024]{2,1,0:T(8,128)(2,1)} %broadcast_in_dim.17), calls=%async_computation | async-start | bytes 5242880 | tf_op jit(solution)/shard_map/all_to_all | solution.py:19
  15.2 131.2 %all-gather.4 = f16[18432,256]{1,0:T(8,128)(2,1)} all-gather(f16[288,256]{1,0:T(8,128)(2,1)S(1)} %convert_element_type.93), channel_id=2, replica_groups=mesh['grp'=2,'sp'=64,'tp'=4] {'sp'}, dimensions={0}, use_global_device_ids=true | all-gather | bytes 9584640 | tf_op jit(solution)/shard_map/all_gather | solution.py:239
  146.4 8.2 %slice_convert_fusion = (bf16[64,64,256]{2,1,0:T(8,128)(2,1)}, bf16[64,64,256]{2,1,0:T(8,128)(2,1)}, bf16[64,64,256]{2,1,0:T(8,128)(2,1)}) fusion(f16[64,288,256]{2,1,0:T(8,128)(2,1)} %bitcast.84), kind=kLoop, calls=%fused_computation.1 | loop fusion | flops 3145728 | bytes 12582912 | tf_op jit(solution)/shard_map/convert_element_type | solution.py:243
  154.6 7.1 %shard_map.83 = bf16[4,288,256]{2,1,0:T(8,128)(2,1)} custom-call(s32[1]{0:T(128)} %constant.28.clone.1.order_ref, bf16[4,320,1024]{2,1,0:T(8,128)(2,1)} %copy-done, bf16[4,1024,256]{2,1,0:T(8,128)(2,1)} %bitcast.98, bf16[4,1024,256]{2,1,0:T(8,128)(2,1)} %bitcast.97, f32[2,4096]{1,0:T(2,128)} %gain_ref.3, f32[31,2,256]{2,1,0:T(2,128)} %bitcast.107), custom_call_target="tpu_custom_call" | custom-call | flops 1342177280 | bytes 6815744 | tf_op jit(solution)/shard_map/pallas_call | solution.py:187
  161.7 3.6 %slice_convert_fusion.1 = bf16[64,64,256]{2,1,0:T(8,128)(2,1)} fusion(f16[64,288,256]{2,1,0:T(8,128)(2,1)} %bitcast.85), kind=kLoop, calls=%fused_computation.2 | loop fusion | flops 1048576 | bytes 4194304 | tf_op jit(solution)/shard_map/convert_element_type | solution.py:243
  165.3 2.6 slice_convert_fusion.4
  167.9 4.8 %all-to-all-start.1 = ((bf16[4,288,256]{2,1,0:T(8,128)(2,1)}), bf16[4,288,256]{2,1,0:T(8,128)(2,1)S(1)}, u32[]{:S(2)}, u32[]{:S(2)}) async-start(bf16[4,288,256]{2,1,0:T(8,128)(2,1)} %shard_map.83), calls=%async_computation.1 | async-start | bytes 1179648 | tf_op jit(solution)/shard_map/all_to_all | solution.py:262
  172.8 2.0 collective-permute-start.2
  174.7 4.0 %collective-permute-start.3 = (bf16[64,32,256]{2,1,0:T(8,128)(2,1)}, bf16[64,32,256]{2,1,0:T(8,128)(2,1)}, u32[]{:S(2)}, u32[]{:S(2)}) collective-permute-start(bf16[64,32,256]{2,1,0:T(8,128)(2,1)} %slice_convert_fusion.4), channel_id=1, source_target_pairs={{0,256},{256,0},{1,257},{257,1},{2,258},{258,2},{3,259},{259,3},{4... | collective-permute-start | bytes 3145736 | tf_op jit(solution)/shard_map/ppermute | solution.py:261
  178.7 2.9 %fusion.40 = (bf16[64,16,256]{2,1,0:T(8,128)(2,1)}, bf16[64,16,256]{2,1,0:T(8,128)(2,1)}, bf16[64,16,256]{2,1,0:T(8,128)(2,1)}, bf16[64,16,256]{2,1,0:T(8,128)(2,1)}) fusion(bf16[64,64,256]{2,1,0:T(8,128)(2,1)} %slice_convert_fusion.1), kind=kLoop, calls=%fused_computation.71 | loop fusion | bytes 4194304 | tf_op jit(solution)/shard_map/slice | solution.py:108
  181.6 1.8 all-to-all-done.1
  183.6 0.3 fusion.4
  184.0 0.5 fusion.29
  184.5 0.5 copy-done.7
  185.0 0.3 fusion.48
  185.3 0.2 copy-done.6
  185.5 0.3 fusion.47
  185.8 0.2 copy-done.5
  186.1 0.3 fusion.46
  186.4 0.2 copy-done.4
  186.6 0.3 fusion.45
  186.9 1.1 multiply_convert_fusion.1
  188.0 22.7 %all-gather.5 = f16[1152,1024]{1,0:T(8,128)(2,1)S(1)} all-gather(f16[288,1024]{1,0:T(8,128)(2,1)S(1)} %get-tuple-element.19), channel_id=3, replica_groups=mesh['grp'=2,'sp'=64,'tp'=4] {'tp'}, dimensions={0}, use_global_device_ids=true | all-gather | bytes 2949120 | tf_op jit(solution)/shard_map/all_gather | solution.py:275
  210.7 2.1 multiply_convert_fusion
  212.8 10.5 %collective-permute-done.2 = bf16[64,64,256]{2,1,0:T(8,128)(2,1)} collective-permute-done((bf16[64,64,256]{2,1,0:T(8,128)(2,1)S(1)}, bf16[64,64,256]{2,1,0:T(8,128)(2,1)}, u32[]{:S(2)}, u32[]{:S(2)}) %collective-permute-start.2) | collective-permute-done | bytes 2097184 | tf_op jit(solution)/shard_map/ppermute | solution.py:247
  223.3 6.8 %shard_map.84 = bf16[4,256,256]{2,1,0:T(8,128)(2,1)} custom-call(s32[1]{0:T(128)} %bitcast.order_ref, bf16[4,288,1024]{2,1,0:T(8,128)(2,1)} %bitcast.95, bf16[4,1024,256]{2,1,0:T(8,128)(2,1)} %bitcast.96, bf16[4,1024,256]{2,1,0:T(8,128)(2,1)} %bitcast.17.b_ref, f32[2,4096]{1,0:T(2,128)} %gain_ref.3, f32[31,2,256]{2,1,0:T(2,128)} %bitcast.108), custom_call_target="tpu_custom_call" | custom-call | flops 1207959552 | bytes 6553600 | tf_op jit(solution)/shard_map/pallas_call | solution.py:187
  230.1 4.9 %all-to-all-start.2 = ((bf16[4,256,256]{2,1,0:T(8,128)(2,1)}), bf16[4,256,256]{2,1,0:T(8,128)(2,1)S(1)}, u32[]{:S(2)}, u32[]{:S(2)}) async-start(bf16[4,256,256]{2,1,0:T(8,128)(2,1)} %shard_map.84), calls=%async_computation.2 | async-start | bytes 1048576 | tf_op jit(solution)/shard_map/all_to_all | solution.py:279
  235.1 9.8 %collective-permute-done.3 = bf16[64,32,256]{2,1,0:T(8,128)(2,1)} collective-permute-done((bf16[64,32,256]{2,1,0:T(8,128)(2,1)}, bf16[64,32,256]{2,1,0:T(8,128)(2,1)}, u32[]{:S(2)}, u32[]{:S(2)}) %collective-permute-start.3) | collective-permute-done | bytes 1048608 | tf_op jit(solution)/shard_map/ppermute | solution.py:261
  244.9 1.3 fusion.42
  246.4 0.3 fusion.16
  246.7 0.5 fusion.24
  247.1 0.2 copy.36
  247.3 0.3 fusion.52
  247.7 0.3 fusion.51
  248.0 0.3 fusion.50
  248.3 0.3 fusion.49
  248.8 0.9 copy-done.3
  249.8 0.2 fusion.25
  250.0 9.6 %all_to_all.21 = f32[4,1,256]{2,1,0:T(1,128)S(1)} all-to-all(f32[4,1,256]{2,1,0:T(1,128)S(1)} %broadcast_in_dim.19), channel_id=1, replica_groups=mesh['grp'=2,'sp'=64,'tp'=4] {'tp'}, dimensions={0} | all-to-all | bytes 8192 | tf_op jit(solution)/shard_map/all_to_all | solution.py:19
  259.7 1.0 fusion.27
  (42 shorter events, 1.1 us)
Async XLA Ops:
  0.0 7.5 %copy-start.8 = (bf16[256,1024]{1,0:T(8,128)(2,1)S(1)}, bf16[256,1024]{1,0:T(8,128)(2,1)}, u32[]{:S(2)}) copy-start(bf16[256,1024]{1,0:T(8,128)(2,1)} %param.8) | copy-start | bytes 1572868
  0.9 6.5 %collective-permute-start = (bf16[32,1024]{1,0:T(8,128)(2,1)S(1)}, bf16[32,1024]{1,0:T(8,128)(2,1)S(1)}, u32[]{:S(2)}, u32[]{:S(2)}) collective-permute-start(bf16[32,1024]{1,0:T(8,128)(2,1)S(1)} %get-tuple-element.37), channel_id=1, source_target_pairs={{0,4},{4,8},{8,12},{12,16},{16,20},{20,24},{24,28},{28,32},{32,36}... | collective-permute-start | bytes 196616 | tf_op jit(solution)/shard_map/ppermute | solution.py:33
  2.8 5.7 %collective-permute-start.1 = (bf16[32,1024]{1,0:T(8,128)(2,1)S(1)}, bf16[32,1024]{1,0:T(8,128)(2,1)S(1)}, u32[]{:S(2)}, u32[]{:S(2)}) collective-permute-start(bf16[32,1024]{1,0:T(8,128)(2,1)S(1)} %get-tuple-element.36), channel_id=1, source_target_pairs={{4,0},{8,4},{12,8},{16,12},{20,16},{24,20},{28,24},{32,28},{36,32}... | collective-permute-start | bytes 196616 | tf_op jit(solution)/shard_map/ppermute | solution.py:34
  10.6 135.8 %all-to-all-start = ((bf16[4,320,1024]{2,1,0:T(8,128)(2,1)}), bf16[4,320,1024]{2,1,0:T(8,128)(2,1)S(1)}, u32[]{:S(2)}, u32[]{:S(2)}) async-start(bf16[4,320,1024]{2,1,0:T(8,128)(2,1)} %broadcast_in_dim.17), calls=%async_computation | async-start | bytes 5242880 | tf_op jit(solution)/shard_map/all_to_all | solution.py:19
  146.4 8.2 %copy-start = (bf16[4,320,1024]{2,1,0:T(8,128)(2,1)}, bf16[4,320,1024]{2,1,0:T(8,128)(2,1)S(1)}, u32[]{:S(2)}) copy-start(bf16[4,320,1024]{2,1,0:T(8,128)(2,1)S(1)} %all-to-all-done.x_ref) | copy-start | bytes 7864324
  165.3 7.5 %copy-start.1 = (bf16[64,64,256]{2,1,0:T(8,128)(2,1)S(1)}, bf16[64,64,256]{2,1,0:T(8,128)(2,1)}, u32[]{:S(2)}) copy-start(bf16[64,64,256]{2,1,0:T(8,128)(2,1)} %get-tuple-element.21) | copy-start | bytes 6291460
  167.9 15.5 %all-to-all-start.1 = ((bf16[4,288,256]{2,1,0:T(8,128)(2,1)}), bf16[4,288,256]{2,1,0:T(8,128)(2,1)S(1)}, u32[]{:S(2)}, u32[]{:S(2)}) async-start(bf16[4,288,256]{2,1,0:T(8,128)(2,1)} %shard_map.83), calls=%async_computation.1 | async-start | bytes 1179648 | tf_op jit(solution)/shard_map/all_to_all | solution.py:262
  172.8 50.5 %collective-permute-start.2 = (bf16[64,64,256]{2,1,0:T(8,128)(2,1)S(1)}, bf16[64,64,256]{2,1,0:T(8,128)(2,1)}, u32[]{:S(2)}, u32[]{:S(2)}) collective-permute-start(bf16[64,64,256]{2,1,0:T(8,128)(2,1)S(1)} %copy-done.1), channel_id=1, source_target_pairs={{0,256},{256,0},{1,257},{257,1},{2,258},{258,2},{3,259},{259,3},{4... | collective-permute-start | bytes 6291464 | tf_op jit(solution)/shard_map/ppermute | solution.py:247
  174.7 70.2 %collective-permute-start.3 = (bf16[64,32,256]{2,1,0:T(8,128)(2,1)}, bf16[64,32,256]{2,1,0:T(8,128)(2,1)}, u32[]{:S(2)}, u32[]{:S(2)}) collective-permute-start(bf16[64,32,256]{2,1,0:T(8,128)(2,1)} %slice_convert_fusion.4), channel_id=1, source_target_pairs={{0,256},{256,0},{1,257},{257,1},{2,258},{258,2},{3,259},{259,3},{4... | collective-permute-start | bytes 3145736 | tf_op jit(solution)/shard_map/ppermute | solution.py:261
  183.9 1.1 copy-start.7
  184.4 1.1 copy-start.6
  185.0 1.1 copy-start.5
  185.5 1.1 copy-start.4
  230.1 4.9 %copy-start.2 = (bf16[64,32,256]{2,1,0:T(8,128)(2,1)S(1)}, bf16[64,32,256]{2,1,0:T(8,128)(2,1)}, u32[]{:S(2)}) copy-start(bf16[64,32,256]{2,1,0:T(8,128)(2,1)} %slice_convert_fusion.4) | copy-start | bytes 3145732
  230.1 16.1 %all-to-all-start.2 = ((bf16[4,256,256]{2,1,0:T(8,128)(2,1)}), bf16[4,256,256]{2,1,0:T(8,128)(2,1)S(1)}, u32[]{:S(2)}, u32[]{:S(2)}) async-start(bf16[4,256,256]{2,1,0:T(8,128)(2,1)} %shard_map.84), calls=%async_computation.2 | async-start | bytes 1048576 | tf_op jit(solution)/shard_map/all_to_all | solution.py:279
  248.7 1.1 copy-start.3
  248.8 10.8 %copy-start.9 = (f32[1024]{0:T(1024)S(1)}, f32[1024]{0:T(1024)}, u32[]{:S(2)}) copy-start(f32[1024]{0:T(1024)} %param.15) | copy-start | bytes 12292

commit v5 on v4

--- a/solution.py
+++ b/solution.py
@@ -57,9 +57,6 @@
             at += rows
         starts = range(0, features, channels)
         blocks = [out_ref[layer, :, i : i + channels].astype(jnp.float32) * OUT_SCALE for i in starts]
-        if paired and layer == LAYERS - 1:
-            middle = len(blocks) // 2
-            blocks = [jnp.where(upper, h, l) for l, h in zip(blocks[:middle], blocks[middle:])]
         for block in blocks:
             sent_ref[at : at + out_rows] = block.astype(jnp.bfloat16)
             at += out_rows
@@ -82,8 +79,7 @@
         for _ in range(1 if paired and layer == LAYERS - 1 else 2):
             of_layer.append(slice(at, at + rows))
             at += rows
-        share = 2 if paired and layer == LAYERS - 1 else 1
-        of_layer.append(slice(at, at + out_rows * (features // channels) // share))
+        of_layer.append(slice(at, at + out_rows * (features // channels)))
         at = of_layer[-1].stop
         slices.append(of_layer)
     vmem = pl.BlockSpec(memory_space=pltpu.VMEM)
@@ -237,7 +233,6 @@
     everyone = exchanged(jnp.concatenate([coded[:1], x_local[1:-1], coded[1:]], axis=0), "tp")
     x_local = x_local[margin:-margin]
     weights = lax.all_gather(sent.astype(jnp.float16), "sp")
-    weights, everyone = lax.optimization_barrier((weights, everyone))
 
     def taken(at):
         return weights[:, at].astype(jnp.bfloat16)
@@ -256,9 +251,6 @@
         middle,
     )
     conv, weights = lax.optimization_barrier((conv, weights))
-    late_outs = [taken(slices[1][-1])]
-    if paired:
-        late_outs.append(lax.ppermute(late_outs[0], "grp", swap))
     conv_all = joined(lax.all_to_all(conv, "tp", 0, 0, tiled=True))
     gains = jnp.concatenate([everyone[:, 0], everyone[:, -1]], axis=1)[:, : 3 * channel_gain.size]
     gains = gains.reshape(-1, LAYERS, 3, channel_gain.shape[1]).astype(jnp.float32)
@@ -276,13 +268,10 @@
     conv = convolved(
         x_all.astype(jnp.bfloat16), late_blocks, order, norm_gain, conv_taps, 1, rows
     )
+    conv, weights = lax.optimization_barrier((conv, weights))
     conv_all = joined(lax.all_to_all(conv, "tp", 0, 0, tiled=True))
     act = activated(conv_all, gains[1])
-    branches = [out_product(act, o, out_rows) for o in late_outs]
-    if paired:
-        own, other = branches
-        branches = [jnp.where(order == 0, own, other), jnp.where(order == 0, other, own)]
-    branch = jnp.concatenate(branches, axis=1)
+    branch = out_product(act, taken(slices[1][-1]), out_rows)
     x_last = (x_next[margin : margin + rows].astype(jnp.float32) + branch).astype(jnp.bfloat16)
 
     xf = x_last.astype(jnp.float32)

time: 262 us -> 243 us (0.927)
  waiting for transfers between devices: 23.1 us -> 13.2 us
  other arithmetic: 22 us -> 15.7 us
  starting transfers between devices: 23.4 us -> 18.2 us
  blocking collectives: 163 us -> 166 us
    ppermute x1, waiting for transfers between devices: 10.5 us -> 0.01 us  [on_device(): late_blocks.append(lax.ppermute(late_blocks[0], 'grp', swap))]
    all_to_all x2, waiting for transfers between devices: 1.81 us -> 12.3 us  [on_device(): conv_all = joined(lax.all_to_all(conv, 'tp', 0, 0, tiled=True))]
    ppermute x1 -> x0, waiting for transfers between devices: 9.8 us -> none  [on_device(): late_outs.append(lax.ppermute(late_outs[0], 'grp', swap))]
    convert_element_type x3, other arithmetic: 14.4 us -> 8.96 us  [taken(): return weights[:, at].astype(jnp.bfloat16)]
    all_gather x1, blocking collectives: 131 us -> 135 us  [on_device(): weights = lax.all_gather(sent.astype(jnp.float16), 'sp')]
    ppermute x1 -> x0, starting transfers between devices: 3.95 us -> none  [on_device(): late_outs.append(lax.ppermute(late_outs[0], 'grp', swap))]
    slice x3 -> x2, local copies, waits for them, and re-layouts: 4.25 us -> 1.17 us  [out_product(): block[:, i:i + rows].reshape(parts * rows, width)]
  transfers between devices with their start and end apart: 7 -> 6, of which waited for: 4 -> 3; matrix products, arithmetic and copies ran while one was open for 4% -> 7% of each run, Pallas kernels for 3% -> 4%
where the time goes in v5:
time: 243 us; the launch traced here: 241 us
  blocking collectives  166 us (68%)
  starting transfers between devices  18.2 us (7%)
  other arithmetic  15.7 us (6%)
  Pallas kernels  15.4 us (6%)
  waiting for transfers between devices  13.2 us (5%)
  local copies, waits for them, and re-layouts  8.71 us (4%)
  matrix products  3.66 us (2%)
    all_gather x1, blocking collectives, on_device(): weights = lax.all_gather(sent.astype(jnp.float16), 'sp')  135 us
    all_gather x1, blocking collectives, on_device(): x_all = lax.all_gather(shared, 'tp').astype(jnp.float32) * (1 / X_SCALE)  22.7 us
    pallas_call x2, Pallas kernels, convolved(): pl.pallas_call(functools.partial(convolved_kernel, first, layer), grid=(c...  13.8 us
    all_to_all x2, waiting for transfers between devices, on_device(): conv_all = joined(lax.all_to_all(conv, 'tp', 0, 0, tiled=True))  12.3 us
    convert_element_type x3, other arithmetic, taken(): return weights[:, at].astype(jnp.bfloat16)  8.96 us
    all_to_all x2, starting transfers between devices, on_device(): conv_all = joined(lax.all_to_all(conv, 'tp', 0, 0, tiled=True))  8.54 us
    all_to_all x1, blocking collectives, exchanged(): lax.all_to_all(jnp.broadcast_to(value[None], (size, *value.shape)), axis,...  7.67 us
  transfers between devices with their start and end apart: 6, of which 3 were waited for; matrix products, arithmetic and copies ran while one was open for 7% of the time, Pallas kernels for 4%

profile of v5, /device:TPU:40, one launch (start us, length us, event | category | flops | bytes accessed | tf_op | source)
XLA Modules:
  0.0 241.0 jit_solution(13215716286490005464)
XLA Ops:
  0.0 0.9 fusion.41
  0.9 1.8 collective-permute-start
  2.8 1.3 collective-permute-start.1
  4.1 1.6 shard_map.82
  5.7 0.8 fusion.42
  6.5 0.9 convert_element_type.93
  7.5 0.9 collective-permute-done.1
  8.5 0.2 slice.115
  8.6 0.2 pad_maximum_fusion
  8.8 1.8 broadcast_in_dim.17
  10.7 4.6 %all-to-all-start = ((bf16[4,320,1024]{2,1,0:T(8,128)(2,1)}), bf16[4,320,1024]{2,1,0:T(8,128)(2,1)S(1)}, u32[]{:S(2)}, u32[]{:S(2)}) async-start(bf16[4,320,1024]{2,1,0:T(8,128)(2,1)} %broadcast_in_dim.17), calls=%async_computation | async-start | bytes 5242880 | tf_op jit(solution)/shard_map/all_to_all | solution.py:19
  15.2 135.3 %all-gather.4 = f16[20480,256]{1,0:T(8,128)(2,1)S(1)} all-gather(f16[320,256]{1,0:T(8,128)(2,1)S(1)} %convert_element_type.93), channel_id=2, replica_groups=mesh['grp'=2,'sp'=64,'tp'=4] {'sp'}, dimensions={0}, use_global_device_ids=true | all-gather | bytes 10649600 | tf_op jit(solution)/shard_map/all_gather | solution.py:235
  150.6 4.7 %slice_convert_fusion = (bf16[64,64,256]{2,1,0:T(8,128)(2,1)}, bf16[64,64,256]{2,1,0:T(8,128)(2,1)}, bf16[64,64,256]{2,1,0:T(8,128)(2,1)}) fusion(f16[64,320,256]{2,1,0:T(8,128)(2,1)S(1)} %bitcast.84), kind=kLoop, calls=%fused_computation.1 | loop fusion | flops 3145728 | bytes 12582912 | tf_op jit(solution)/shard_map/convert_element_type | solution.py:238
  155.3 1.1 copy-done
  156.3 1.9 collective-permute-start.2
  158.3 1.5 copy-done.1
  159.8 7.1 %shard_map.83 = bf16[4,288,256]{2,1,0:T(8,128)(2,1)} custom-call(s32[1]{0:T(128)} %constant.50.clone.1.order_ref, bf16[4,320,1024]{2,1,0:T(8,128)(2,1)} %copy-done.1, bf16[4,1024,256]{2,1,0:T(8,128)(2,1)} %bitcast.97, bf16[4,1024,256]{2,1,0:T(8,128)(2,1)} %bitcast.96, f32[2,4096]{1,0:T(2,128)} %gain_ref.3, f32[31,2,256]{2,1,0:T(2,128)} %bitcast.106), custom_call_target="tpu_custom_call" | custom-call | flops 1342177280 | bytes 6815744 | tf_op jit(solution)/shard_map/pallas_call | solution.py:183
  166.9 4.8 %all-to-all-start.1 = ((bf16[4,288,256]{2,1,0:T(8,128)(2,1)}), bf16[4,288,256]{2,1,0:T(8,128)(2,1)S(1)}, u32[]{:S(2)}, u32[]{:S(2)}) async-start(bf16[4,288,256]{2,1,0:T(8,128)(2,1)} %shard_map.83), calls=%async_computation.1 | async-start | bytes 1179648 | tf_op jit(solution)/shard_map/all_to_all | solution.py:254
  171.7 0.9 fusion.38
  172.7 2.1 slice_convert_fusion.4
  174.8 0.2 fusion.40
  175.0 7.4 %all-to-all-done.1 = bf16[4,288,256]{2,1,0:T(8,128)(2,1)S(1)} async-done(((bf16[4,288,256]{2,1,0:T(8,128)(2,1)}), bf16[4,288,256]{2,1,0:T(8,128)(2,1)S(1)}, u32[]{:S(2)}, u32[]{:S(2)}) %all-to-all-start.1) | async-done | bytes 589856 | tf_op jit(solution)/shard_map/all_to_all | solution.py:254
  182.4 0.2 convert_reduce_fusion
  182.6 0.3 fusion.4
  182.9 0.5 fusion.30
  183.5 0.3 fusion.46
  183.8 0.3 fusion.45
  184.2 0.3 fusion.44
  184.5 0.3 fusion.43
  184.8 0.3 multiply_convert_fusion.1
  185.1 22.7 %all-gather.5 = f16[1152,1024]{1,0:T(8,128)(2,1)S(1)} all-gather(f16[288,1024]{1,0:T(8,128)(2,1)S(1)} %get-tuple-element.19), channel_id=3, replica_groups=mesh['grp'=2,'sp'=64,'tp'=4] {'tp'}, dimensions={0}, use_global_device_ids=true | all-gather | bytes 2949120 | tf_op jit(solution)/shard_map/all_gather | solution.py:267
  207.8 2.1 multiply_convert_fusion
  209.9 6.8 %shard_map.84 = bf16[4,256,256]{2,1,0:T(8,128)(2,1)} custom-call(s32[1]{0:T(128)} %bitcast.order_ref, bf16[4,288,1024]{2,1,0:T(8,128)(2,1)} %bitcast.95, bf16[4,1024,256]{2,1,0:T(8,128)(2,1)} %bitcast.16.a_ref, bf16[4,1024,256]{2,1,0:T(8,128)(2,1)} %bitcast.17.b_ref, f32[2,4096]{1,0:T(2,128)} %gain_ref.3, f32[31,2,256]{2,1,0:T(2,128)} %bitcast.107), custom_call_target="tpu_custom_call" | custom-call | flops 1207959552 | bytes 6553600 | tf_op jit(solution)/shard_map/pallas_call | solution.py:183
  216.7 3.7 %all-to-all-start.2 = ((bf16[4,256,256]{2,1,0:T(8,128)(2,1)}), bf16[4,256,256]{2,1,0:T(8,128)(2,1)S(1)}, u32[]{:S(2)}, u32[]{:S(2)}) async-start(bf16[4,256,256]{2,1,0:T(8,128)(2,1)} %shard_map.84), calls=%async_computation.2 | async-start | bytes 1048576 | tf_op jit(solution)/shard_map/all_to_all | solution.py:272
  220.4 2.1 slice_convert_fusion.3
  222.6 1.0 fusion.39
  223.5 4.9 %all-to-all-done.2 = bf16[4,256,256]{2,1,0:T(8,128)(2,1)S(1)} async-done(((bf16[4,256,256]{2,1,0:T(8,128)(2,1)}), bf16[4,256,256]{2,1,0:T(8,128)(2,1)S(1)}, u32[]{:S(2)}, u32[]{:S(2)}) %all-to-all-start.2) | async-done | bytes 524320 | tf_op jit(solution)/shard_map/all_to_all | solution.py:272
  228.5 0.1 convert_reduce_fusion.1
  228.6 0.3 fusion.16
  228.9 0.5 fusion.24
  229.4 0.2 copy.36
  229.6 1.4 fusion.50
  231.0 0.3 fusion.49
  231.3 0.3 fusion.48
  231.6 0.3 fusion.47
  232.0 0.3 fusion.25
  232.3 7.7 %all_to_all.21 = f32[4,1,256]{2,1,0:T(1,128)S(1)} all-to-all(f32[4,1,256]{2,1,0:T(1,128)S(1)} %broadcast_in_dim.19), channel_id=1, replica_groups=mesh['grp'=2,'sp'=64,'tp'=4] {'tp'}, dimensions={0} | all-to-all | bytes 8192 | tf_op jit(solution)/shard_map/all_to_all | solution.py:19
  240.0 1.0 fusion.27
  (26 shorter events, 0.2 us)
Async XLA Ops:
  0.0 7.5 %copy-start.2 = (bf16[256,1024]{1,0:T(8,128)(2,1)S(1)}, bf16[256,1024]{1,0:T(8,128)(2,1)}, u32[]{:S(2)}) copy-start(bf16[256,1024]{1,0:T(8,128)(2,1)} %param.8) | copy-start | bytes 1572868
  0.9 6.5 %collective-permute-start = (bf16[32,1024]{1,0:T(8,128)(2,1)S(1)}, bf16[32,1024]{1,0:T(8,128)(2,1)S(1)}, u32[]{:S(2)}, u32[]{:S(2)}) collective-permute-start(bf16[32,1024]{1,0:T(8,128)(2,1)S(1)} %get-tuple-element.35), channel_id=1, source_target_pairs={{0,4},{4,8},{8,12},{12,16},{16,20},{20,24},{24,28},{28,32},{32,36}... | collective-permute-start | bytes 196616 | tf_op jit(solution)/shard_map/ppermute | solution.py:33
  2.8 5.7 %collective-permute-start.1 = (bf16[32,1024]{1,0:T(8,128)(2,1)S(1)}, bf16[32,1024]{1,0:T(8,128)(2,1)S(1)}, u32[]{:S(2)}, u32[]{:S(2)}) collective-permute-start(bf16[32,1024]{1,0:T(8,128)(2,1)S(1)} %get-tuple-element.34), channel_id=1, source_target_pairs={{4,0},{8,4},{12,8},{16,12},{20,16},{24,20},{28,24},{32,28},{36,32}... | collective-permute-start | bytes 196616 | tf_op jit(solution)/shard_map/ppermute | solution.py:34
  10.7 147.6 %all-to-all-start = ((bf16[4,320,1024]{2,1,0:T(8,128)(2,1)}), bf16[4,320,1024]{2,1,0:T(8,128)(2,1)S(1)}, u32[]{:S(2)}, u32[]{:S(2)}) async-start(bf16[4,320,1024]{2,1,0:T(8,128)(2,1)} %broadcast_in_dim.17), calls=%async_computation | async-start | bytes 5242880 | tf_op jit(solution)/shard_map/all_to_all | solution.py:19
  150.6 5.8 %copy-start = (f16[20480,256]{1,0:T(8,128)(2,1)}, f16[20480,256]{1,0:T(8,128)(2,1)S(1)}, u32[]{:S(2)}) copy-start(f16[20480,256]{1,0:T(8,128)(2,1)S(1)} %all-gather.4) | copy-start | bytes 31457284
  156.3 53.6 %collective-permute-start.2 = (bf16[64,64,256]{2,1,0:T(8,128)(2,1)}, bf16[64,64,256]{2,1,0:T(8,128)(2,1)}, u32[]{:S(2)}, u32[]{:S(2)}) collective-permute-start(bf16[64,64,256]{2,1,0:T(8,128)(2,1)} %get-tuple-element.21), channel_id=1, source_target_pairs={{0,256},{256,0},{1,257},{257,1},{2,258},{258,2},{3,259},{259,3},{4... | collective-permute-start | bytes 6291464 | tf_op jit(solution)/shard_map/ppermute | solution.py:242
  158.3 1.5 copy-start.1
  166.9 15.5 %all-to-all-start.1 = ((bf16[4,288,256]{2,1,0:T(8,128)(2,1)}), bf16[4,288,256]{2,1,0:T(8,128)(2,1)S(1)}, u32[]{:S(2)}, u32[]{:S(2)}) async-start(bf16[4,288,256]{2,1,0:T(8,128)(2,1)} %shard_map.83), calls=%async_computation.1 | async-start | bytes 1179648 | tf_op jit(solution)/shard_map/all_to_all | solution.py:254
  216.7 11.8 %all-to-all-start.2 = ((bf16[4,256,256]{2,1,0:T(8,128)(2,1)}), bf16[4,256,256]{2,1,0:T(8,128)(2,1)S(1)}, u32[]{:S(2)}, u32[]{:S(2)}) async-start(bf16[4,256,256]{2,1,0:T(8,128)(2,1)} %shard_map.84), calls=%async_computation.2 | async-start | bytes 1048576 | tf_op jit(solution)/shard_map/all_to_all | solution.py:272
  232.0 8.0 %copy-start.3 = (f32[1024]{0:T(1024)S(1)}, f32[1024]{0:T(1024)}, u32[]{:S(2)}) copy-start(f32[1024]{0:T(1024)} %param.15) | copy-start | bytes 12292

commit v6 on v5

--- a/solution.py
+++ b/solution.py
@@ -57,6 +57,8 @@
             at += rows
         starts = range(0, features, channels)
         blocks = [out_ref[layer, :, i : i + channels].astype(jnp.float32) * OUT_SCALE for i in starts]
+        if paired and layer == LAYERS - 1:
+            blocks = [*blocks[:-2], jnp.where(upper, blocks[-1], blocks[-2])]
         for block in blocks:
             sent_ref[at : at + out_rows] = block.astype(jnp.bfloat16)
             at += out_rows
@@ -79,7 +81,8 @@
         for _ in range(1 if paired and layer == LAYERS - 1 else 2):
             of_layer.append(slice(at, at + rows))
             at += rows
-        of_layer.append(slice(at, at + out_rows * (features // channels)))
+        spared = 1 if paired and layer == LAYERS - 1 else 0
+        of_layer.append(slice(at, at + out_rows * (features // channels - spared)))
         at = of_layer[-1].stop
         slices.append(of_layer)
     vmem = pl.BlockSpec(memory_space=pltpu.VMEM)
@@ -251,6 +254,11 @@
         middle,
     )
     conv, weights = lax.optimization_barrier((conv, weights))
+    late_out = slices[1][-1]
+    if paired:
+        late_out = slice(late_out.start, late_out.stop - out_rows)
+        own_out = taken(slice(late_out.stop, late_out.stop + out_rows))
+        other_out = lax.ppermute(own_out, "grp", swap)
     conv_all = joined(lax.all_to_all(conv, "tp", 0, 0, tiled=True))
     gains = jnp.concatenate([everyone[:, 0], everyone[:, -1]], axis=1)[:, : 3 * channel_gain.size]
     gains = gains.reshape(-1, LAYERS, 3, channel_gain.shape[1]).astype(jnp.float32)
@@ -271,7 +279,11 @@
     conv, weights = lax.optimization_barrier((conv, weights))
     conv_all = joined(lax.all_to_all(conv, "tp", 0, 0, tiled=True))
     act = activated(conv_all, gains[1])
-    branch = out_product(act, taken(slices[1][-1]), out_rows)
+    branch = out_product(act, taken(late_out), out_rows)
+    if paired:
+        own, other = [out_product(act, o, out_rows) for o in (own_out, other_out)]
+        last_two = jnp.where(order == 0, own, other), jnp.where(order == 0, other, own)
+        branch = jnp.concatenate([branch, *last_two], axis=1)
     x_last = (x_next[margin : margin + rows].astype(jnp.float32) + branch).astype(jnp.bfloat16)
 
     xf = x_last.astype(jnp.float32)

time: 243 us -> 247 us (1.016)
  starting transfers between devices: 18.2 us -> 22.4 us
  blocking collectives: 166 us -> 163 us
  local copies, waits for them, and re-layouts: 8.71 us -> 11.3 us
    ppermute x0 -> x1, starting transfers between devices: none -> 3.95 us  [on_device(): other_out = lax.ppermute(own_out, 'grp', swap)]
    all_gather x1, blocking collectives: 135 us -> 133 us  [on_device(): weights = lax.all_gather(sent.astype(jnp.float16), 'sp')]
    unnamed x11 -> x21, local copies, waits for them, and re-layouts: 2.65 us -> 5.05 us
    convert_element_type x3 -> x4, other arithmetic: 8.96 us -> 9.45 us  [taken(): return weights[:, at].astype(jnp.bfloat16)]
  transfers between devices with their start and end apart: 6 -> 7, of which waited for: 3 -> 3; matrix products, arithmetic and copies ran while one was open for 7% -> 8% of each run, Pallas kernels for 4% -> 6%
where the time goes in v6:
time: 247 us; the launch traced here: 244 us
  blocking collectives  163 us (66%)
  starting transfers between devices  22.4 us (9%)
  other arithmetic  16.2 us (7%)
  Pallas kernels  15.4 us (6%)
  waiting for transfers between devices  11.8 us (5%)
  local copies, waits for them, and re-layouts  11.3 us (5%)
  matrix products  3.69 us (1%)
    all_gather x1, blocking collectives, on_device(): weights = lax.all_gather(sent.astype(jnp.float16), 'sp')  133 us
    all_gather x1, blocking collectives, on_device(): x_all = lax.all_gather(shared, 'tp').astype(jnp.float32) * (1 / X_SCALE)  22.7 us
    pallas_call x2, Pallas kernels, convolved(): pl.pallas_call(functools.partial(convolved_kernel, first, layer), grid=(c...  13.8 us
    all_to_all x2, waiting for transfers between devices, on_device(): conv_all = joined(lax.all_to_all(conv, 'tp', 0, 0, tiled=True))  10.9 us
    convert_element_type x4, other arithmetic, taken(): return weights[:, at].astype(jnp.bfloat16)  9.45 us
    all_to_all x2, starting transfers between devices, on_device(): conv_all = joined(lax.all_to_all(conv, 'tp', 0, 0, tiled=True))  8.76 us
    all_to_all x1, blocking collectives, exchanged(): lax.all_to_all(jnp.broadcast_to(value[None], (size, *value.shape)), axis,...  7.67 us
    unnamed x21, local copies, waits for them, and re-layouts  5.05 us
  transfers between devices with their start and end apart: 7, of which 3 were waited for; matrix products, arithmetic and copies ran while one was open for 8% of the time, Pallas kernels for 6%

profile of v6, /device:TPU:40, one launch (start us, length us, event | category | flops | bytes accessed | tf_op | source)
XLA Modules:
  0.0 244.4 jit_solution(8281394645089906724)
XLA Ops:
  0.0 0.9 fusion.40
  0.9 1.8 collective-permute-start
  2.8 1.3 collective-permute-start.1
  4.1 1.6 shard_map.82
  5.7 0.8 fusion.41
  6.5 0.9 convert_element_type.96
  7.5 0.9 collective-permute-done.1
  8.8 1.8 broadcast_in_dim.17
  10.6 4.6 %all-to-all-start = ((bf16[4,320,1024]{2,1,0:T(8,128)(2,1)}), bf16[4,320,1024]{2,1,0:T(8,128)(2,1)S(1)}, u32[]{:S(2)}, u32[]{:S(2)}) async-start(bf16[4,320,1024]{2,1,0:T(8,128)(2,1)} %broadcast_in_dim.17), calls=%async_computation | async-start | bytes 5242880 | tf_op jit(solution)/shard_map/all_to_all | solution.py:19
  15.2 132.8 %all-gather.4 = f16[19456,256]{1,0:T(8,128)(2,1)S(1)} all-gather(f16[304,256]{1,0:T(8,128)(2,1)S(1)} %convert_element_type.96), channel_id=2, replica_groups=mesh['grp'=2,'sp'=64,'tp'=4] {'sp'}, dimensions={0}, use_global_device_ids=true | all-gather | bytes 10117120 | tf_op jit(solution)/shard_map/all_gather | solution.py:238
  148.0 3.9 %slice_convert_fusion = (bf16[64,64,256]{2,1,0:T(8,128)(2,1)}, bf16[64,64,256]{2,1,0:T(8,128)(2,1)}, bf16[64,64,256]{2,1,0:T(8,128)(2,1)}) fusion(f16[64,304,256]{2,1,0:T(8,128)(2,1)S(1)} %bitcast.84), kind=kLoop, calls=%fused_computation.1 | loop fusion | flops 3145728 | bytes 12582912 | tf_op jit(solution)/shard_map/convert_element_type | solution.py:241
  151.9 1.8 copy-done
  153.7 1.9 collective-permute-start.2
  155.7 1.5 copy-done.1
  157.2 7.1 %shard_map.83 = bf16[4,288,256]{2,1,0:T(8,128)(2,1)} custom-call(s32[1]{0:T(128)} %constant.27.clone.1.order_ref, bf16[4,320,1024]{2,1,0:T(8,128)(2,1)} %copy-done.1, bf16[4,1024,256]{2,1,0:T(8,128)(2,1)} %bitcast.94, bf16[4,1024,256]{2,1,0:T(8,128)(2,1)} %bitcast.93, f32[2,4096]{1,0:T(2,128)} %gain_ref.3, f32[31,2,256]{2,1,0:T(2,128)} %bitcast.106), custom_call_target="tpu_custom_call" | custom-call | flops 1342177280 | bytes 6815744 | tf_op jit(solution)/shard_map/pallas_call | solution.py:186
  164.2 2.1 slice_convert_fusion.3
  166.4 1.9 slice_convert_fusion.5
  168.3 5.0 %all-to-all-start.1 = ((bf16[4,288,256]{2,1,0:T(8,128)(2,1)}), bf16[4,288,256]{2,1,0:T(8,128)(2,1)S(1)}, u32[]{:S(2)}, u32[]{:S(2)}) async-start(bf16[4,288,256]{2,1,0:T(8,128)(2,1)} %shard_map.83), calls=%async_computation.1 | async-start | bytes 1179648 | tf_op jit(solution)/shard_map/all_to_all | solution.py:262
  173.3 0.9 fusion.37
  174.3 4.0 %collective-permute-start.3 = (bf16[64,16,256]{2,1,0:T(8,128)(2,1)}, bf16[64,16,256]{2,1,0:T(8,128)(2,1)}, u32[]{:S(2)}, u32[]{:S(2)}) collective-permute-start(bf16[64,16,256]{2,1,0:T(8,128)(2,1)} %slice_convert_fusion.5), channel_id=1, source_target_pairs={{0,256},{256,0},{1,257},{257,1},{2,258},{258,2},{3,259},{259,3},{4... | collective-permute-start | bytes 1572872 | tf_op jit(solution)/shard_map/ppermute | solution.py:261
  178.3 1.3 fusion.38
  179.6 4.4 %all-to-all-done.1 = bf16[4,288,256]{2,1,0:T(8,128)(2,1)S(1)} async-done(((bf16[4,288,256]{2,1,0:T(8,128)(2,1)}), bf16[4,288,256]{2,1,0:T(8,128)(2,1)S(1)}, u32[]{:S(2)}, u32[]{:S(2)}) %all-to-all-start.1) | async-done | bytes 589856 | tf_op jit(solution)/shard_map/all_to_all | solution.py:262
  184.2 0.3 fusion.4
  184.6 0.5 fusion.29
  185.1 0.5 copy-done.5
  185.6 0.3 fusion.45
  185.9 0.2 copy-done.4
  186.1 0.3 fusion.44
  186.5 0.2 copy-done.3
  186.7 0.3 fusion.43
  187.2 0.3 fusion.42
  187.5 0.3 multiply_convert_fusion.1
  187.9 22.7 %all-gather.5 = f16[1152,1024]{1,0:T(8,128)(2,1)S(1)} all-gather(f16[288,1024]{1,0:T(8,128)(2,1)S(1)} %get-tuple-element.19), channel_id=3, replica_groups=mesh['grp'=2,'sp'=64,'tp'=4] {'tp'}, dimensions={0}, use_global_device_ids=true | all-gather | bytes 2949120 | tf_op jit(solution)/shard_map/all_gather | solution.py:275
  210.6 2.1 multiply_convert_fusion
  212.6 6.8 %shard_map.84 = bf16[4,256,256]{2,1,0:T(8,128)(2,1)} custom-call(s32[1]{0:T(128)} %bitcast.order_ref, bf16[4,288,1024]{2,1,0:T(8,128)(2,1)} %bitcast.92, bf16[4,1024,256]{2,1,0:T(8,128)(2,1)} %bitcast.16.a_ref, bf16[4,1024,256]{2,1,0:T(8,128)(2,1)} %bitcast.17.b_ref, f32[2,4096]{1,0:T(2,128)} %gain_ref.3, f32[31,2,256]{2,1,0:T(2,128)} %bitcast.107), custom_call_target="tpu_custom_call" | custom-call | flops 1207959552 | bytes 6553600 | tf_op jit(solution)/shard_map/pallas_call | solution.py:186
  219.4 3.7 %all-to-all-start.2 = ((bf16[4,256,256]{2,1,0:T(8,128)(2,1)}), bf16[4,256,256]{2,1,0:T(8,128)(2,1)S(1)}, u32[]{:S(2)}, u32[]{:S(2)}) async-start(bf16[4,256,256]{2,1,0:T(8,128)(2,1)} %shard_map.84), calls=%async_computation.2 | async-start | bytes 1048576 | tf_op jit(solution)/shard_map/all_to_all | solution.py:280
  223.1 1.5 slice_convert_fusion.4
  224.7 6.4 %all-to-all-done.2 = bf16[4,256,256]{2,1,0:T(8,128)(2,1)S(1)} async-done(((bf16[4,256,256]{2,1,0:T(8,128)(2,1)}), bf16[4,256,256]{2,1,0:T(8,128)(2,1)S(1)}, u32[]{:S(2)}, u32[]{:S(2)}) %all-to-all-start.2) | async-done | bytes 524320 | tf_op jit(solution)/shard_map/all_to_all | solution.py:280
  231.3 0.3 fusion.16
  231.6 0.5 fusion.24
  232.3 0.3 fusion.47
  232.6 0.3 fusion.46
  233.0 0.6 copy-done.7
  233.7 0.3 convolution_multiply_fusion.1
  234.0 1.4 broadcast_select_fusion.1
  235.4 0.2 fusion.25
  235.7 7.7 %all_to_all.21 = f32[4,1,256]{2,1,0:T(1,128)S(1)} all-to-all(f32[4,1,256]{2,1,0:T(1,128)S(1)} %broadcast_in_dim.19), channel_id=1, replica_groups=mesh['grp'=2,'sp'=64,'tp'=4] {'tp'}, dimensions={0} | all-to-all | bytes 8192 | tf_op jit(solution)/shard_map/all_to_all | solution.py:19
  243.4 1.0 fusion.27
  (40 shorter events, 1.4 us)
Async XLA Ops:
  0.0 7.5 %copy-start.6 = (bf16[256,1024]{1,0:T(8,128)(2,1)S(1)}, bf16[256,1024]{1,0:T(8,128)(2,1)}, u32[]{:S(2)}) copy-start(bf16[256,1024]{1,0:T(8,128)(2,1)} %param.8) | copy-start | bytes 1572868
  0.9 6.5 %collective-permute-start = (bf16[32,1024]{1,0:T(8,128)(2,1)S(1)}, bf16[32,1024]{1,0:T(8,128)(2,1)S(1)}, u32[]{:S(2)}, u32[]{:S(2)}) collective-permute-start(bf16[32,1024]{1,0:T(8,128)(2,1)S(1)} %get-tuple-element.35), channel_id=1, source_target_pairs={{0,4},{4,8},{8,12},{12,16},{16,20},{20,24},{24,28},{28,32},{32,36}... | collective-permute-start | bytes 196616 | tf_op jit(solution)/shard_map/ppermute | solution.py:33
  2.8 5.7 %collective-permute-start.1 = (bf16[32,1024]{1,0:T(8,128)(2,1)S(1)}, bf16[32,1024]{1,0:T(8,128)(2,1)S(1)}, u32[]{:S(2)}, u32[]{:S(2)}) collective-permute-start(bf16[32,1024]{1,0:T(8,128)(2,1)S(1)} %get-tuple-element.34), channel_id=1, source_target_pairs={{4,0},{8,4},{12,8},{16,12},{20,16},{24,20},{28,24},{32,28},{36,32}... | collective-permute-start | bytes 196616 | tf_op jit(solution)/shard_map/ppermute | solution.py:34
  10.6 145.0 %all-to-all-start = ((bf16[4,320,1024]{2,1,0:T(8,128)(2,1)}), bf16[4,320,1024]{2,1,0:T(8,128)(2,1)S(1)}, u32[]{:S(2)}, u32[]{:S(2)}) async-start(bf16[4,320,1024]{2,1,0:T(8,128)(2,1)} %broadcast_in_dim.17), calls=%async_computation | async-start | bytes 5242880 | tf_op jit(solution)/shard_map/all_to_all | solution.py:19
  148.0 5.7 %copy-start = (f16[19456,256]{1,0:T(8,128)(2,1)}, f16[19456,256]{1,0:T(8,128)(2,1)S(1)}, u32[]{:S(2)}) copy-start(f16[19456,256]{1,0:T(8,128)(2,1)S(1)} %all-gather.4) | copy-start | bytes 29884420
  153.7 58.9 %collective-permute-start.2 = (bf16[64,64,256]{2,1,0:T(8,128)(2,1)}, bf16[64,64,256]{2,1,0:T(8,128)(2,1)}, u32[]{:S(2)}, u32[]{:S(2)}) collective-permute-start(bf16[64,64,256]{2,1,0:T(8,128)(2,1)} %get-tuple-element.21), channel_id=1, source_target_pairs={{0,256},{256,0},{1,257},{257,1},{2,258},{258,2},{3,259},{259,3},{4... | collective-permute-start | bytes 6291464 | tf_op jit(solution)/shard_map/ppermute | solution.py:245
  155.7 1.5 copy-start.1
  168.3 15.7 %all-to-all-start.1 = ((bf16[4,288,256]{2,1,0:T(8,128)(2,1)}), bf16[4,288,256]{2,1,0:T(8,128)(2,1)S(1)}, u32[]{:S(2)}, u32[]{:S(2)}) async-start(bf16[4,288,256]{2,1,0:T(8,128)(2,1)} %shard_map.83), calls=%async_computation.1 | async-start | bytes 1179648 | tf_op jit(solution)/shard_map/all_to_all | solution.py:262
  174.3 59.7 %collective-permute-start.3 = (bf16[64,16,256]{2,1,0:T(8,128)(2,1)}, bf16[64,16,256]{2,1,0:T(8,128)(2,1)}, u32[]{:S(2)}, u32[]{:S(2)}) collective-permute-start(bf16[64,16,256]{2,1,0:T(8,128)(2,1)} %slice_convert_fusion.5), channel_id=1, source_target_pairs={{0,256},{256,0},{1,257},{257,1},{2,258},{258,2},{3,259},{259,3},{4... | collective-permute-start | bytes 1572872 | tf_op jit(solution)/shard_map/ppermute | solution.py:261
  184.5 1.0 copy-start.5
  185.1 1.1 copy-start.4
  185.6 1.1 copy-start.3
  186.1 1.1 copy-start.2
  219.4 11.8 %all-to-all-start.2 = ((bf16[4,256,256]{2,1,0:T(8,128)(2,1)}), bf16[4,256,256]{2,1,0:T(8,128)(2,1)S(1)}, u32[]{:S(2)}, u32[]{:S(2)}) async-start(bf16[4,256,256]{2,1,0:T(8,128)(2,1)} %shard_map.84), calls=%async_computation.2 | async-start | bytes 1048576 | tf_op jit(solution)/shard_map/all_to_all | solution.py:280
  232.6 1.0 copy-start.7
  235.4 8.0 %copy-start.8 = (f32[1024]{0:T(1024)S(1)}, f32[1024]{0:T(1024)}, u32[]{:S(2)}) copy-start(f32[1024]{0:T(1024)} %param.15) | copy-start | bytes 12292
